TPU v7x, 32 devices: a whole 2x2x4 slice. The times are simulated.
32 devices in a mesh: sp: 16 (over z, x, core), tp: 2 (over y).
Axes of the slice: x: 2, y: 2, z: 4, core: 2. Of those that a mesh axis runs over, the one named last changes fastest.
Arguments:
- value_rows: bfloat16 [16384, 1024], P('sp', 'tp'), may hold values from -6 to 6
- gate_rows: bfloat16 [16384, 1024], P('sp', 'tp'), may hold values from -6 to 6
- conv_taps: bfloat16 [31, 1024], P(None, 'tp'), may hold values from -1 to 1
- norm_gain: float32 [1024], P('tp'), may hold values from 0.1 to 1.9
- point_weight: bfloat16 [1024, 1024], P(None, 'tp'), may hold values from -0.1875 to 0.1875
- out_grad: bfloat16 [16384, 1024], P('sp', 'tp'), may hold values from -6 to 6
Outputs:
- value_grad: bfloat16 [16384, 1024], P('sp', 'tp')
- gate_grad: bfloat16 [16384, 1024], P('sp', 'tp')
- taps_grad: float32 [31, 1024], P(None, 'tp')
- gain_grad: float32 [1024], P('tp')
- weight_grad: float32 [1024, 1024], P('sp', 'tp')
All inputs are finite; a program needn't handle non-finite values.
Results may differ from a plain program's by a relative error of at most 0.0051.
Values may be sent and summed in bfloat16 or wider, within the bound.
A program may use at most 128 MiB of HBM per device.

v0:
```python
import jax
import jax.numpy as jnp
from jax import lax
from jax.sharding import PartitionSpec as P

GROUP = 64


EPS = 1e-06


def extended(value, sides, width):
    for axis, dim in sides:
        peers, length = (lax.axis_size(axis), value.shape[dim])
        up = [(i, (i + 1) % peers) for i in range(peers - 1)]
        down = [(j, i) for i, j in up]
        last = lax.slice_in_dim(value, length - width, length, axis=dim)
        initial = lax.slice_in_dim(value, 0, width, axis=dim)
        before = lax.ppermute(last, axis, up)
        after = lax.ppermute(initial, axis, down)
        value = jnp.concatenate([before, value, after], axis=dim)
    return value


def per_device(value_rows, gate_rows, conv_taps, norm_gain, point_weight, out_grad):
    row_count = value_rows.shape[0]
    chan_count = value_rows.shape[1]
    tap_count = conv_taps.shape[0]
    half_width = tap_count // 2
    groups = chan_count // GROUP
    gate_sig = jax.nn.sigmoid(gate_rows.astype(jnp.float32))
    value_f = value_rows.astype(jnp.float32)
    gated = (value_f * gate_sig).astype(jnp.bfloat16)
    margin = 0
    gated_wide = extended(gated, (("sp", 0),), half_width)
    extent = row_count + 2 * margin
    taps_f = conv_taps.astype(jnp.float32)
    convolved = jnp.zeros((extent, chan_count), jnp.float32)
    for tap_index in range(tap_count):
        convolved = convolved + taps_f[tap_index] * gated_wide[
            tap_index : tap_index + extent
        ].astype(jnp.float32)
    grouped = convolved.reshape(extent, groups, GROUP)
    group_mean = jnp.mean(grouped, axis=-1, keepdims=True)
    centred = grouped - group_mean
    inv_std = lax.rsqrt(jnp.mean(centred * centred, axis=-1, keepdims=True) + EPS)
    unit_conv = centred * inv_std
    gain_g = norm_gain.reshape(groups, GROUP)
    pre_act = unit_conv * gain_g
    act_sig = jax.nn.sigmoid(pre_act)
    normed = (pre_act * act_sig).astype(jnp.bfloat16).reshape(extent, chan_count)
    full_grad = lax.all_gather(out_grad, "tp", axis=1, tiled=True)
    normed_grad = jnp.dot(full_grad, point_weight, preferred_element_type=jnp.float32).reshape(
        extent, groups, GROUP
    )
    weight_grad = lax.psum_scatter(
        lax.dot_general(
            full_grad, normed, (((0,), (0,)), ((), ())), preferred_element_type=jnp.float32
        ),
        "sp",
        scatter_dimension=0,
        tiled=True,
    )
    act_grad = normed_grad * act_sig * (1.0 + pre_act * (1.0 - act_sig))
    gain_part = jnp.sum(act_grad * unit_conv, axis=0).reshape(chan_count)
    hat_grad = act_grad * gain_g
    conv_grad = inv_std * (
        hat_grad
        - jnp.mean(hat_grad, axis=-1, keepdims=True)
        - unit_conv * jnp.mean(hat_grad * unit_conv, axis=-1, keepdims=True)
    )
    conv_grad = conv_grad.reshape(extent, chan_count)
    grad_wide = extended(conv_grad, (("sp", 0),), half_width)
    taps_part = jnp.stack(
        [
            jnp.sum(
                conv_grad
                * gated_wide[margin + tap_index : margin + tap_index + row_count].astype(
                    jnp.float32
                ),
                axis=0,
            )
            for tap_index in range(tap_count)
        ]
    )
    taps_grad, gain_grad = lax.psum((taps_part, gain_part), "sp")
    gated_grad = jnp.zeros((row_count, chan_count), jnp.float32)
    for tap_index in range(tap_count):
        lower = 2 * half_width - tap_index
        gated_grad = gated_grad + taps_f[tap_index] * grad_wide[lower : lower + row_count]
    value_grad = (gated_grad * gate_sig).astype(jnp.bfloat16)
    gate_grad = (gated_grad * value_f * gate_sig * (1.0 - gate_sig)).astype(jnp.bfloat16)
    return (value_grad, gate_grad, taps_grad, gain_grad, weight_grad)


def solution(mesh):
    return jax.shard_map(
        per_device,
        mesh=mesh,
        in_specs=(
            P("sp", "tp"),
            P("sp", "tp"),
            P(None, "tp"),
            P("tp"),
            P(None, "tp"),
            P("sp", "tp"),
        ),
        out_specs=(P("sp", "tp"), P("sp", "tp"), P(None, "tp"), P("tp"), P("sp", "tp")),
        check_vma=False,
    )
```

profile of v0, /device:TPU:0, one launch (start us, length us, event | category | flops | bytes accessed | tf_op | source)
XLA Modules:
  0.0 248.2 jit_solution(14803031081066323375)
XLA Ops:
  8.0 2.2 fusion
  10.2 2.4 collective-permute-start
  14.2 3.6 %collective-permute-done.1 = bf16[15,512]{1,0:T(8,128)(2,1)S(1)} collective-permute-done((bf16[15,512]{1,0:T(8,128)(2,1)S(1)}, bf16[15,512]{1,0:T(8,128)(2,1)S(1)}, u32[]{:S(2)}, u32[]{:S(2)}) %collective-permute-start.1) | collective-permute-done | bytes 15392 | tf_op jit(solution)/shard_map/ppermute | solution.py:20
  17.8 14.0 %fusion.59 = f32[1024,512]{1,0:T(8,128)} fusion(bf16[1024,512]{1,0:T(8,128)(2,1)S(1)} %fusion, bf16[15,512]{1,0:T(8,128)(2,1)S(1)} %collective-permute-done.1, bf16[15,512]{1,0:T(8,128)(2,1)S(1)} %collective-permute-done, f32[512]{0:T(512)S(1)} %bitcast.156, f32[512]{0:T(512)S(1)} %bitcast.154, f32[512]{0:T(512)S(1)} %bitcast.152, f32[512]{0:T(512)S(1)} %bitcast.150, ...), kind=kLoop, calls=%fused_computation.179 | loop fusion | flops 95420416 | bytes 3239936 | tf_op jit(solution)/shard_map/add | solution.py:40
  36.0 2.9 %copy.28 = f32[1024,512]{1,0:T(8,128)} copy(f32[1024,512]{0,1:T(8,128)} %bitcast.90) | data formatting | bytes 4194304 | tf_op jit(solution)/shard_map/mul | solution.py:67
  40.5 2.9 %copy.23 = f32[1024,512]{1,0:T(8,128)} copy(f32[1024,512]{0,1:T(8,128)} %bitcast.91) | data formatting | bytes 4194304 | tf_op jit(solution)/shard_map/sub | solution.py:45
  43.4 2.0 all-gather.2.cloned.1.call-done
  45.4 7.9 %multiply_reduce_fusion = (f32[512]{0:T(512)}, f32[1024,512]{1,0:T(8,128)}, f32[1024,512]{1,0:T(8,128)}) fusion(f32[512]{0:T(512)S(1)} %copy-done.19, f32[1024,512]{1,0:T(8,128)} %copy.28, f32[1024,512]{1,0:T(8,128)} %fusion.59, f32[1024,512]{1,0:T(8,128)} %copy.23, bf16[1024,1024]{1,0:T(8,128)(2,1)} %all-gather.2.cloned.1.call-done, ...), kind=kOutput, calls=%fused_computation.299 | convolution fusion | flops 1080557056 | bytes 13635584 | tf_op jit(solution)/shard_map/dot_general | solution.py:53
  53.3 2.9 %copy.25 = f32[1024,512]{0,1:T(8,128)} copy(f32[1024,512]{1,0:T(8,128)} %get-tuple-element.99) | data formatting | bytes 4194304 | tf_op jit(solution)/shard_map/dot_general | solution.py:53
  56.2 4.1 %fusion.185 = (f32[1024,8]{0,1:T(8,128)S(1)}, f32[1024,8]{0,1:T(8,128)S(1)}, f32[1024,8,64]{0,2,1:T(8,128)}) fusion(f32[1024,8]{0,1:T(8,128)S(1)} %add_rsqrt_fusion, f32[1024,8]{0,1:T(8,128)S(1)} %broadcast_multiply_fusion.2, f32[1024,512]{0,1:T(8,128)S(1)} %copy.22, f32[8,64]{1,0:T(8,128)S(1)} %mul.807, f32[1024,512]{0,1:T(8,128)} %copy.25), kind=kLoop, calls=%fused_computation.349 | loop fusion | flops 7847936 | bytes 6424576 | tf_op jit(solution)/shard_map/reduce_sum | solution.py:69
  64.6 7.9 %fusion.63 = (f32[512]{0:T(512)S(1)}, f32[512]{0:T(512)S(1)}, f32[512]{0:T(512)S(1)}, f32[512]{0:T(512)S(1)}, f32[512]{0:T(512)S(1)}, /*index=5*/f32[512]{0:T(512)S(1)}, f32[1024,512]{1,0:T(8,128)S(1)}) fusion(bf16[15,512]{1,0:T(8,128)(2,1)S(1)} %collective-permute-done.1, bf16[1024,512]{1,0:T(8,128)(2,1)} %copy-done.3, f32[1024,512]{1,0:T(8,128)} %copy.28, ...), kind=kLoop, calls=%fused_computation.183 | loop fusion | flops 26211328 | bytes 13661184 | tf_op jit(solution)/shard_map/reduce_sum | solution.py:76
  72.5 2.1 fusion.47
  74.6 2.4 fusion.64
  78.7 2.1 fusion.43
  80.8 2.5 %stack.127 = f32[31,512]{1,0:T(8,128)} concatenate(f32[1,512]{1,0:T(1,128)S(1)} %bitcast.167, f32[1,512]{1,0:T(1,128)S(1)} %bitcast.168, f32[1,512]{1,0:T(1,128)S(1)} %bitcast.169, f32[1,512]{1,0:T(1,128)S(1)} %bitcast.175, f32[1,512]{1,0:T(1,128)S(1)} %bitcast.174, f32[1,512]{1,0:T(1,128)S(1)} %bitcast.173, f32[1,512]{1,0:T(1,128)S(1)} %bitcast.172, f32[1,512]{1,0:T(1,128)S(1)} %bitcast.171, ...), dimensions={0} | concatenate | bytes 126976 | tf_op jit(solution)/shard_map/stack | solution.py:74
  83.4 5.0 %convolution_bitcast_fusion = f32[1024,512]{0,1:T(8,128)} fusion(bf16[1024,1024]{1,0:T(8,128)(2,1)} %all-gather.2.cloned.1.call-done, f32[1024,512]{1,0:T(8,128)} %get-tuple-element.59, f32[512]{0:T(512)S(1)} %copy-done.19), kind=kOutput, calls=%fused_computation.311 | convolution fusion | flops 1076887552 | bytes 6293504 | tf_op jit(solution)/shard_map/dot_general | solution.py:57
  88.4 1.9 subtract_multiply_fusion
  90.4 2.9 %copy.34 = f32[1024,512]{1,0:T(8,128)} copy(f32[1024,512]{0,1:T(8,128)} %convolution_bitcast_fusion) | data formatting | bytes 4194304
  96.3 2.5 collective-permute-start.3
  100.1 2.4 collective-permute-done.2
  102.5 15.9 %fusion.3 = (bf16[1024,512]{1,0:T(8,128)(2,1)}, f32[1024,512]{1,0:T(8,128)}) fusion(bf16[1024,512]{1,0:T(8,128)(2,1)} %param.6, bf16[1024,512]{1,0:T(8,128)(2,1)} %param.7, f32[1024,512]{1,0:T(8,128)S(1)} %get-tuple-element.60, f32[15,512]{1,0:T(8,128)S(1)} %collective-permute-done.3, f32[512]{0:T(512)} %bitcast.157, f32[512]{0:T(512)} %bitcast.155, ...), kind=kLoop, calls=%fused_computation.123 | loop fusion | flops 52953088 | bytes 7464960 | tf_op jit(solution)/shard_map/convert_element_type | solution.py:92
  118.5 3.2 %multiply_convert_fusion.1 = bf16[1024,512]{1,0:T(8,128)(2,1)} fusion(f32[1024,512]{1,0:T(8,128)} %get-tuple-element.62, bf16[1024,512]{1,0:T(8,128)(2,1)S(1)} %copy-done.5), kind=kLoop, calls=%fused_computation.300 | loop fusion | flops 3145728 | bytes 4194304 | tf_op jit(solution)/shard_map/convert_element_type | solution.py:91
  121.6 49.6 %all-reduce.3.cloned.1.call-done = (f32[31,512]{1,0:T(8,128)}, f32[512]{0:T(512)}) async-done(((f32[31,512]{1,0:T(8,128)}, f32[512]{0:T(512)}), (f32[31,512]{1,0:T(8,128)}, f32[512]{0:T(512)})) %all-reduce.3.cloned.1.call-update) | async-done | bytes 65552 | tf_op jit(solution)/shard_map/psum | solution.py:86
  171.2 67.7 %reduce-scatter.4.cloned.1.call-done = f32[64,512]{1,0:T(8,128)} async-done(((f32[1024,512]{1,0:T(8,128)}), f32[64,512]{1,0:T(8,128)}) %reduce-scatter.4.cloned.1.call-update) | async-done | bytes 131088
  (72 shorter events, 21.0 us)
Async XLA Ops:
  7.2 38.2 %copy-start = (bf16[1024,512]{1,0:T(8,128)(2,1)S(1)}, bf16[1024,512]{1,0:T(8,128)(2,1)}, u32[]{:S(2)}) copy-start(bf16[1024,512]{1,0:T(8,128)(2,1)} %param.10) | copy-start | bytes 3145732
  7.2 6.8 %copy-start.19 = (f32[512]{0:T(512)S(1)}, f32[512]{0:T(512)}, u32[]{:S(2)}) copy-start(f32[512]{0:T(512)} %param.9) | copy-start | bytes 6148
  7.2 38.2 %all-gather.2.cloned.1.call-start = ((), (), s32[]{:S(2)}) async-start(), calls=%async_computation.1 | async-start | bytes 3145728 | tf_op jit(solution)/shard_map/all_gather | solution.py:52
  7.9 163.3 %all-reduce.3.cloned.1.call-start = ((), (), s32[]{:S(2)}) async-start(), calls=%async_computation.3 | async-start | bytes 135168 | tf_op jit(solution)/shard_map/psum | solution.py:86
  10.2 7.6 %copy-start.3 = (bf16[1024,512]{1,0:T(8,128)(2,1)}, bf16[1024,512]{1,0:T(8,128)(2,1)S(1)}, u32[]{:S(2)}) copy-start(bf16[1024,512]{1,0:T(8,128)(2,1)S(1)} %fusion) | copy-start | bytes 3145732
  10.2 4.0 %collective-permute-start = (bf16[15,512]{1,0:T(8,128)(2,1)S(1)}, bf16[15,512]{1,0:T(8,128)(2,1)S(1)}, u32[]{:S(2)}, u32[]{:S(2)}) collective-permute-start(bf16[15,512]{1,0:T(8,128)(2,1)S(1)} %get-tuple-element.66), channel_id=1, source_target_pairs={{0,2},{2,4},{4,6},{6,8},{8,10},{10,12},{12,14},{14,16},{16,18},{18... | collective-permute-start | bytes 46088 | tf_op jit(solution)/shard_map/ppermute | solution.py:19
  12.6 5.2 %collective-permute-start.1 = (bf16[15,512]{1,0:T(8,128)(2,1)S(1)}, bf16[15,512]{1,0:T(8,128)(2,1)S(1)}, u32[]{:S(2)}, u32[]{:S(2)}) collective-permute-start(bf16[15,512]{1,0:T(8,128)(2,1)S(1)} %get-tuple-element.67), channel_id=1, source_target_pairs={{2,0},{4,2},{6,4},{8,6},{10,8},{12,10},{14,12},{16,14},{18,16},{20... | collective-permute-start | bytes 46088 | tf_op jit(solution)/shard_map/ppermute | solution.py:20
  14.0 19.7 %copy-start.8 = (f32[1,512]{1,0:T(1,128)}, f32[1,512]{1,0:T(1,128)S(1)}, u32[]{:S(2)}) copy-start(f32[1,512]{1,0:T(1,128)S(1)} %get-tuple-element.88) | copy-start | bytes 6148
  14.0 19.7 %copy-start.9 = (f32[1,512]{1,0:T(1,128)}, f32[1,512]{1,0:T(1,128)S(1)}, u32[]{:S(2)}) copy-start(f32[1,512]{1,0:T(1,128)S(1)} %get-tuple-element.89) | copy-start | bytes 6148
  14.0 19.7 %copy-start.10 = (f32[1,512]{1,0:T(1,128)}, f32[1,512]{1,0:T(1,128)S(1)}, u32[]{:S(2)}) copy-start(f32[1,512]{1,0:T(1,128)S(1)} %get-tuple-element.90) | copy-start | bytes 6148
  14.0 19.7 %copy-start.11 = (f32[1,512]{1,0:T(1,128)}, f32[1,512]{1,0:T(1,128)S(1)}, u32[]{:S(2)}) copy-start(f32[1,512]{1,0:T(1,128)S(1)} %get-tuple-element.91) | copy-start | bytes 6148
  14.0 19.7 %copy-start.12 = (f32[1,512]{1,0:T(1,128)}, f32[1,512]{1,0:T(1,128)S(1)}, u32[]{:S(2)}) copy-start(f32[1,512]{1,0:T(1,128)S(1)} %get-tuple-element.92) | copy-start | bytes 6148
  14.0 19.7 %copy-start.13 = (f32[1,512]{1,0:T(1,128)}, f32[1,512]{1,0:T(1,128)S(1)}, u32[]{:S(2)}) copy-start(f32[1,512]{1,0:T(1,128)S(1)} %get-tuple-element.93) | copy-start | bytes 6148
  14.0 19.7 %copy-start.14 = (f32[1,512]{1,0:T(1,128)}, f32[1,512]{1,0:T(1,128)S(1)}, u32[]{:S(2)}) copy-start(f32[1,512]{1,0:T(1,128)S(1)} %get-tuple-element.94) | copy-start | bytes 6148
  14.0 19.7 %copy-start.15 = (f32[1,512]{1,0:T(1,128)}, f32[1,512]{1,0:T(1,128)S(1)}, u32[]{:S(2)}) copy-start(f32[1,512]{1,0:T(1,128)S(1)} %get-tuple-element.95) | copy-start | bytes 6148
  14.1 19.7 %copy-start.16 = (f32[1,512]{1,0:T(1,128)}, f32[1,512]{1,0:T(1,128)S(1)}, u32[]{:S(2)}) copy-start(f32[1,512]{1,0:T(1,128)S(1)} %get-tuple-element.96) | copy-start | bytes 6148
  14.1 19.7 %copy-start.17 = (f32[1,512]{1,0:T(1,128)}, f32[1,512]{1,0:T(1,128)S(1)}, u32[]{:S(2)}) copy-start(f32[1,512]{1,0:T(1,128)S(1)} %get-tuple-element.97) | copy-start | bytes 6148
  14.1 19.7 %copy-start.18 = (f32[1,512]{1,0:T(1,128)}, f32[1,512]{1,0:T(1,128)S(1)}, u32[]{:S(2)}) copy-start(f32[1,512]{1,0:T(1,128)S(1)} %get-tuple-element.98) | copy-start | bytes 6148
  33.8 22.5 %copy-start.1 = (f32[1024,512]{0,1:T(8,128)}, f32[1024,512]{0,1:T(8,128)S(1)}, u32[]{:S(2)}) copy-start(f32[1024,512]{0,1:T(8,128)S(1)} %copy.22) | copy-start | bytes 6291460
  64.6 7.9 %copy-start.4 = (bf16[1024,512]{1,0:T(8,128)(2,1)S(1)}, bf16[1024,512]{1,0:T(8,128)(2,1)}, u32[]{:S(2)}) copy-start(bf16[1024,512]{1,0:T(8,128)(2,1)} %copy-done.3) | copy-start | bytes 3145732
  83.3 155.6 %reduce-scatter.4.cloned.1.call-start = ((), (), s32[]{:S(2)}) async-start(), calls=%async_computation.2 | async-start | bytes 2228224
  96.3 22.1 %copy-start.5 = (bf16[1024,512]{1,0:T(8,128)(2,1)S(1)}, bf16[1024,512]{1,0:T(8,128)(2,1)}, u32[]{:S(2)}) copy-start(bf16[1024,512]{1,0:T(8,128)(2,1)} %param.7) | copy-start | bytes 3145732
  96.3 3.8 %collective-permute-start.3 = (f32[15,512]{1,0:T(8,128)S(1)}, f32[15,512]{1,0:T(8,128)S(1)}, u32[]{:S(2)}, u32[]{:S(2)}) collective-permute-start(f32[15,512]{1,0:T(8,128)S(1)} %copy.33), channel_id=1, source_target_pairs={{0,2},{2,4},{4,6},{6,8},{8,10},{10,12},{12,14},{14,16},{16,18},{18... | collective-permute-start | bytes 92168 | tf_op jit(solution)/shard_map/ppermute | solution.py:19
  98.8 3.7 %collective-permute-start.2 = (f32[15,512]{1,0:T(8,128)S(1)}, f32[15,512]{1,0:T(8,128)S(1)}, u32[]{:S(2)}, u32[]{:S(2)}) collective-permute-start(f32[15,512]{1,0:T(8,128)S(1)} %copy.32), channel_id=1, source_target_pairs={{2,0},{4,2},{6,4},{8,6},{10,8},{12,10},{14,12},{16,14},{18,16},{20... | collective-permute-start | bytes 92168 | tf_op jit(solution)/shard_map/ppermute | solution.py:20
  (3 other events, 16.8 us)
Sparse Core Ops, SparseCore 0:
  9.6 35.8 all-gather.1
  83.5 87.6 all-reduce.2
  175.5 63.3 reduce-scatter.3
where the time goes:
time: 249 us; the launch traced here: 248 us
  waiting for transfers between devices  126 us (51%)
  other arithmetic  58 us (23%)
  local copies, waits for them, and re-layouts  29.5 us (12%)
  between operations  14.2 us (6%)
  matrix products  12.9 us (5%)
  starting transfers between devices  7.56 us (3%)
    unnamed x4, waiting for transfers between devices  68.4 us
    psum x1, waiting for transfers between devices, per_device(): taps_grad, gain_grad = lax.psum((taps_part, gain_part), 'sp')  49.6 us
    reduce_sum x5, other arithmetic, per_device(): jnp.sum(conv_grad * gated_wide[margin + tap_index:margin + tap_index + ro...  16.1 us
    convert_element_type x1, other arithmetic, per_device(): (gated_grad * value_f * gate_sig * (1.0 - gate_sig)).astype(jnp.bfloat16)  15.9 us
    add x1, other arithmetic, per_device(): convolved + taps_f[tap_index] * gated_wide[tap_index:tap_index + extent]....  14 us
    dot_general x1, matrix products, per_device(): jnp.dot(full_grad, point_weight, preferred_element_type=jnp.float32)  7.9 us
    ppermute x2, waiting for transfers between devices, extended(): after = lax.ppermute(initial, axis, down)  6.03 us
    unnamed x43, local copies, waits for them, and re-layouts  5.76 us
  transfers between devices with their start and end apart: 7, of which 5 were waited for; matrix products, arithmetic and copies ran while one was open for 24% of the time, Pallas kernels for 0%

commit v1 on v0

v1 whole, which is shorter than its diff:
```python
import functools

import jax
import jax.numpy as jnp
from jax import lax
from jax.experimental import pallas as pl
from jax.experimental.pallas import tpu as pltpu
from jax.sharding import PartitionSpec as P

GROUP = 64
EPS = 1e-06
LANE = 128
EDGE = 16
F32, BF16 = jnp.float32, jnp.bfloat16


def sigmoid(x):
    return 0.5 * jnp.tanh(0.5 * x) + 0.5


def divisor(total, *choices):
    for choice in choices:
        if total % choice == 0:
            return choice
    return total


def group_matrix():
    row = lax.broadcasted_iota(jnp.int32, (2 * LANE, LANE), 0)
    col = lax.broadcasted_iota(jnp.int32, (2 * LANE, LANE), 1)
    same = lax.rem(row, LANE) // GROUP == col // GROUP
    return jnp.where(same, 1.0 / GROUP, 0.0).astype(BF16)


def group_mean(x, matrix):
    high = x.astype(BF16)
    low = (x - high.astype(F32)).astype(BF16)
    return jnp.dot(jnp.concatenate([high, low], axis=1), matrix, preferred_element_type=F32)


def lanes(c):
    return pl.ds(pl.multiple_of(c * LANE, LANE), LANE)


def forward(value, gate, vlo, vhi, glo, ghi, taps, gain, gated, unit, inv, normed):
    rows, chans = value.shape
    tiles = chans // LANE
    kw = taps.shape[1]
    extent = unit.shape[1]
    matrix = group_matrix()

    def gate_tile(c, _):
        def put(v_ref, g_ref, src, n, dst):
            v = v_ref[pl.ds(src, n), lanes(c)].astype(F32)
            g = g_ref[pl.ds(src, n), lanes(c)].astype(F32)
            gated[c, pl.ds(dst, n), :] = (v * sigmoid(g)).astype(BF16).astype(F32)

        put(vlo, glo, 0, 2 * EDGE, 0)
        put(vhi, ghi, 0, 2 * EDGE, rows + 2 * EDGE)
        step = divisor(rows, 256, 32)

        def chunk(r, _):
            at = pl.multiple_of(r * step, step)
            put(value, gate, at, step, pl.multiple_of(at + 2 * EDGE, 8))
            return 0

        lax.fori_loop(0, rows // step, chunk, 0)

        cstep = divisor(extent, 96, 32)

        def conv(r, _):
            at = r * cstep
            acc = jnp.zeros((cstep, LANE), F32)
            for k in range(kw):
                acc += taps[c, pl.ds(k, 1), :] * gated[c, pl.ds(at + (k + 2 * EDGE - EDGE - kw // 2), cstep), :]
            unit[c, pl.ds(pl.multiple_of(at, 8), cstep), :] = acc
            return 0

        lax.fori_loop(0, extent // cstep, conv, 0)

        nstep = divisor(extent, 352, 32)

        def norm(r, _):
            at = pl.multiple_of(r * nstep, 8)
            x = unit[c, pl.ds(at, nstep), :]
            centred = x - group_mean(x, matrix)
            rs = lax.rsqrt(group_mean(centred * centred, matrix) + EPS)
            inv[c, pl.ds(at, nstep), :] = rs
            unit[c, pl.ds(at, nstep), :] = centred * rs
            return 0

        lax.fori_loop(0, extent // nstep, norm, 0)

        def act(r, _):
            at = pl.multiple_of(r * step, step)
            p = unit[c, pl.ds(pl.multiple_of(at + EDGE, 8), step), :] * gain[:, lanes(c)]
            normed[pl.ds(at, step), lanes(c)] = (p * sigmoid(p)).astype(BF16)
            return 0

        lax.fori_loop(0, rows // step, act, 0)
        return 0

    lax.fori_loop(0, tiles, gate_tile, 0)


def middle(grad, others, elo, ehi, weight, unit, inv, normed, gain, dconv, gain_part, wpart):
    rows, chans = grad.shape
    tiles = chans // LANE
    peers = others.shape[0] + 1
    me = lax.axis_index("tp")
    matrix = group_matrix()
    step = divisor(rows, 256, 32)
    gain_part[...] = jnp.zeros_like(gain_part)

    def owner(j):
        return pl.ds(pl.multiple_of(lax.rem(me + j, peers) * chans, chans), chans)

    def finish(ng, at, n, own):
        for c in range(tiles):
            g = gain[:, c * LANE:(c + 1) * LANE]
            u = unit[c, pl.ds(at, n), :]
            p = u * g
            s = sigmoid(p)
            a = ng[:, c * LANE:(c + 1) * LANE] * s * (1.0 + p * (1.0 - s))
            au = a * u
            if own:
                gain_part[:, c * LANE:(c + 1) * LANE] += jnp.sum(au.reshape(n // 8, 8, LANE), axis=0)
            h = a * g
            hu = au * g
            dconv[c, pl.ds(at, n), :] = inv[c, pl.ds(at, n), :] * (
                h - group_mean(h, matrix) - u * group_mean(hu, matrix))

    for ref, at in ((elo, 0), (ehi, rows + EDGE)):
        ng = sum(jnp.dot(ref[j], weight[owner(j), :], preferred_element_type=F32) for j in range(peers))
        finish(ng, at, EDGE, False)

    def chunk(r, _):
        at = pl.multiple_of(r * step, step)
        ng = jnp.dot(grad[pl.ds(at, step), :], weight[owner(0), :], preferred_element_type=F32)
        for j in range(1, peers):
            ng += jnp.dot(others[j - 1, pl.ds(at, step), :], weight[owner(j), :], preferred_element_type=F32)
        finish(ng, pl.multiple_of(at + EDGE, 8), step, True)
        return 0

    lax.fori_loop(0, rows // step, chunk, 0)

    piece = divisor(chans, 256, 128)
    for j in range(peers):
        def cols(q, _):
            src = pl.ds(pl.multiple_of(q * piece, piece), piece)
            lhs = grad[:, src] if j == 0 else others[j - 1, :, src]
            out = lax.dot_general(lhs, normed[...], (((0,), (0,)), ((), ())), preferred_element_type=F32)
            base = lax.rem(me + j, peers) * chans
            wpart[pl.ds(pl.multiple_of(base + q * piece, piece), piece), :] = out
            return 0

        lax.fori_loop(0, chans // piece, cols, 0)


def taps_body(dconv, gated, sums):
    tiles, kw1 = sums.shape[0], sums.shape[1]
    kw = kw1 - 1
    rows = dconv.shape[1] - 2 * EDGE

    def tile(c, _):
        def chunk(r, accs):
            at = r * 16
            out = []
            d0 = dconv[c, pl.ds(pl.multiple_of(at + EDGE, 8), 8), :]
            d1 = dconv[c, pl.ds(pl.multiple_of(at + EDGE + 8, 8), 8), :]
            for k in range(kw):
                g0 = gated[c, pl.ds(at + (k + 2 * EDGE - kw // 2), 8), :]
                g1 = gated[c, pl.ds(at + (k + 2 * EDGE - kw // 2 + 8), 8), :]
                out.append(accs[k] + (d0 * g0 + d1 * g1))
            return tuple(out)

        accs = lax.fori_loop(0, rows // 16, chunk, tuple(jnp.zeros((8, LANE), F32) for _ in range(kw)))
        for k in range(kw):
            sums[c, pl.ds(k, 1), :] = jnp.sum(accs[k], axis=0, keepdims=True)
        return 0

    lax.fori_loop(0, tiles, tile, 0)


def taps_kernel(dconv, gated, gain_part, sums):
    taps_body(dconv, gated, sums)
    kw = sums.shape[1] - 1
    for c in range(sums.shape[0]):
        sums[c, pl.ds(kw, 1), :] = jnp.sum(gain_part[:, c * LANE:(c + 1) * LANE], axis=0, keepdims=True)


def backward(dconv, value, gate, taps, vgrad, ggrad):
    rows, chans = value.shape
    tiles = chans // LANE
    kw = taps.shape[1]
    step = divisor(rows, 64, 32)

    def tile(c, _):
        def chunk(r, _):
            at = pl.multiple_of(r * step, step)
            acc = jnp.zeros((step, LANE), F32)
            for k in range(kw):
                acc += taps[c, pl.ds(k, 1), :] * dconv[c, pl.ds(at + (EDGE + kw // 2 - k), step), :]
            s = sigmoid(gate[pl.ds(at, step), lanes(c)].astype(F32))
            v = value[pl.ds(at, step), lanes(c)].astype(F32)
            gs = acc * s
            vgrad[pl.ds(at, step), lanes(c)] = gs.astype(BF16)
            ggrad[pl.ds(at, step), lanes(c)] = (gs * v * (1.0 - s)).astype(BF16)
            return 0

        lax.fori_loop(0, rows // step, chunk, 0)
        return 0

    lax.fori_loop(0, tiles, tile, 0)


def call(body, outs, args, flops, bytes_accessed):
    return pl.pallas_call(
        body,
        out_shape=[jax.ShapeDtypeStruct(s, d) for s, d in outs],
        in_specs=[pl.BlockSpec(memory_space=pltpu.VMEM)] * len(args),
        out_specs=[pl.BlockSpec(memory_space=pltpu.VMEM)] * len(outs),
        compiler_params=pltpu.CompilerParams(vmem_limit_bytes=48 * 1024 * 1024),
        cost_estimate=pl.CostEstimate(flops=flops, bytes_accessed=bytes_accessed, transcendentals=0),
    )(*args)


def per_device(value, gate, conv_taps, norm_gain, point_weight, out_grad):
    rows, chans = value.shape
    kw = conv_taps.shape[0]
    tiles = chans // LANE
    n, peers = lax.axis_size("sp"), lax.axis_size("tp")
    extent = rows + 2 * EDGE
    up = [(i, i + 1) for i in range(n - 1)]
    down = [(j, i) for i, j in up]
    swap = [[((t + j) % peers, t) for t in range(peers)] for j in range(1, peers)]

    both = jnp.stack([value[-2 * EDGE:], gate[-2 * EDGE:]]), jnp.stack([value[:2 * EDGE], gate[:2 * EDGE]])
    lo = lax.ppermute(both[0], "sp", up)
    hi = lax.ppermute(both[1], "sp", down)
    edges = jnp.stack([out_grad[-EDGE:], out_grad[:EDGE]])
    elo = lax.ppermute(edges[0], "sp", up)
    ehi = lax.ppermute(edges[1], "sp", down)
    ends = jnp.stack([elo, ehi])
    ends = jnp.stack([ends] + [lax.ppermute(ends, "tp", s) for s in swap])
    others = jnp.stack([lax.ppermute(out_grad, "tp", s) for s in swap])
    taps = conv_taps.astype(F32).reshape(kw, tiles, LANE).transpose(1, 0, 2)
    gain = norm_gain.reshape(1, chans)

    big = rows * chans
    gated, unit, inv, normed = call(
        forward,
        [((tiles, rows + 4 * EDGE, LANE), F32), ((tiles, extent, LANE), F32), ((tiles, extent, LANE), F32), ((rows, chans), BF16)],
        [value, gate, lo[0], hi[0], lo[1], hi[1], taps, gain], 2 * kw * big, 20 * big)
    dconv, gain_part, wpart = call(
        middle,
        [((tiles, extent, LANE), F32), ((8, chans), F32), ((peers * chans, chans), F32)],
        [out_grad, others, ends[:, 0], ends[:, 1], point_weight, unit, inv, normed, gain], 8 * big * peers * chans // 2, 20 * big)
    (sums,) = call(taps_kernel, [((tiles, kw + 1, LANE), F32)], [dconv, gated, gain_part], 2 * kw * big, 20 * big)
    vgrad, ggrad = call(backward, [((rows, chans), BF16)] * 2, [dconv, value, gate, taps], 2 * kw * big, 20 * big)

    me = lax.axis_index("sp")
    w = wpart.reshape(n, peers * chans // n, chans)
    bit = 1
    while bit < n:
        pairs = [(i, i ^ bit) for i in range(n)]
        mine = (me // bit) % 2
        halves = w.reshape(w.shape[0] // 2, 2, *w.shape[1:])
        keep = lax.dynamic_index_in_dim(halves, mine, 1, keepdims=False)
        send = lax.dynamic_index_in_dim(halves, 1 - mine, 1, keepdims=False)
        w = keep + lax.ppermute(send.astype(BF16), "sp", pairs).astype(F32)
        sums = sums + lax.ppermute(sums, "sp", pairs)
        bit *= 2
    flat = sums.transpose(1, 0, 2).reshape(kw + 1, chans)
    return vgrad, ggrad, flat[:kw], flat[kw], w[0]


def solution(mesh):
    return jax.shard_map(
        per_device,
        mesh=mesh,
        in_specs=(P("sp", "tp"), P("sp", "tp"), P(None, "tp"), P("tp"), P(None, "tp"), P("sp", "tp")),
        out_specs=(P("sp", "tp"), P("sp", "tp"), P(None, "tp"), P("tp"), P("sp", "tp")),
        check_vma=False,
    )
```

time: 249 us -> 99.2 us (0.40)
  waiting for transfers between devices: 126 us -> 19.6 us
  other arithmetic: 58 us -> 4.28 us
  Pallas kernels: 0 us -> 38.5 us
  local copies, waits for them, and re-layouts: 29.5 us -> 14.1 us
  starting transfers between devices: 7.56 us -> 21 us
  between operations: 14.2 us -> 1 us
  matrix products: 12.9 us -> 0 us
    unnamed x4 -> x0, waiting for transfers between devices: 68.4 us -> none
    psum x1 -> x0, waiting for transfers between devices: 49.6 us -> none  [per_device(): taps_grad, gain_grad = lax.psum((taps_part, gain_part), 'sp')]
    pallas_call x0 -> x4, Pallas kernels: none -> 38.5 us  [call(): pl.pallas_call(body, out_shape=[jax.ShapeDtypeStruct(s, d) for s, d in ou...]
    convert_element_type x3 -> x0, other arithmetic: 21.3 us -> none  [the longest x1 15.9 us: per_device(): (gated_grad * value_f * gate_sig * (1.0 - gate_sig)).astype(jnp.bfloat16)]
    reduce_sum x8 -> x0, other arithmetic: 20.8 us -> none  [the longest x5 16.1 us: per_device(): jnp.sum(conv_grad * gated_wide[margin + tap_index:margin + tap_index + ro...]
    ppermute x4 -> x14, starting transfers between devices: 7.44 us -> 21 us  [the longest x4 4.74 us: per_device(): sums = sums + lax.ppermute(sums, 'sp', pairs)]
    ppermute x4 -> x14, waiting for transfers between devices: 6.03 us -> 19.6 us  [the longest x1 12.4 us: per_device(): ends = jnp.stack([ends] + [lax.ppermute(ends, 'tp', s) for s in swap])]
    dot_general x2 -> x0, matrix products: 12.9 us -> none  [the longest x1 7.9 us: per_device(): jnp.dot(full_grad, point_weight, preferred_element_type=jnp.float32)]
  transfers between devices with their start and end apart: 7 -> 14, of which waited for: 5 -> 6; matrix products, arithmetic and copies ran while one was open for 24% -> 6% of each run, Pallas kernels for 0% -> 29%
where the time goes in v1:
time: 99.2 us; the launch traced here: 98.5 us
  Pallas kernels  38.5 us (39%)
  starting transfers between devices  21 us (21%)
  waiting for transfers between devices  19.6 us (20%)
  local copies, waits for them, and re-layouts  14.1 us (14%)
  other arithmetic  4.28 us (4%)
  between operations  1 us (1%)
    pallas_call x4, Pallas kernels, call(): pl.pallas_call(body, out_shape=[jax.ShapeDtypeStruct(s, d) for s, d in ou...  38.5 us
    ppermute x1, waiting for transfers between devices, per_device(): ends = jnp.stack([ends] + [lax.ppermute(ends, 'tp', s) for s in swap])  12.4 us
    unnamed x28, local copies, waits for them, and re-layouts  8.83 us
    ppermute x4, starting transfers between devices, per_device(): sums = sums + lax.ppermute(sums, 'sp', pairs)  4.74 us
    ppermute x4, starting transfers between devices, per_device(): w = keep + lax.ppermute(send.astype(BF16), 'sp', pairs).astype(F32)  4.05 us
    ppermute x4, waiting for transfers between devices, per_device(): w = keep + lax.ppermute(send.astype(BF16), 'sp', pairs).astype(F32)  3.99 us
    add x3, other arithmetic, per_device(): w = keep + lax.ppermute(send.astype(BF16), 'sp', pairs).astype(F32)  3.54 us
    ppermute x4, waiting for transfers between devices, per_device(): sums = sums + lax.ppermute(sums, 'sp', pairs)  3.25 us
  transfers between devices with their start and end apart: 14, of which 6 were waited for; matrix products, arithmetic and copies ran while one was open for 6% of the time, Pallas kernels for 29%

profile of v1, /device:TPU:0, one launch (start us, length us, event | category | flops | bytes accessed | tf_op | source)
XLA Modules:
  0.0 98.5 jit_solution(9940174850719710633)
XLA Ops:
  0.6 3.1 %collective-permute-start = (bf16[1024,512]{1,0:T(8,128)(2,1)}, bf16[1024,512]{1,0:T(8,128)(2,1)S(1)}, u32[]{:S(2)}, u32[]{:S(2)}) collective-permute-start(bf16[1024,512]{1,0:T(8,128)(2,1)} %grad.1), channel_id=1, source_target_pairs={{1,0},{0,1},{3,2},{2,3},{5,4},{4,5},{7,6},{6,7},{9,8},{8,9},{11,10... | collective-permute-start | bytes 3145736 | tf_op jit(solution)/shard_map/ppermute | solution.py:246
  4.5 1.3 %collective-permute-start.2 = (bf16[16,512]{1,0:T(8,128)(2,1)S(1)}, bf16[16,512]{1,0:T(8,128)(2,1)S(1)}, u32[]{:S(2)}, u32[]{:S(2)}) collective-permute-start(bf16[16,512]{1,0:T(8,128)(2,1)S(1)} %get-tuple-element.28), channel_id=1, source_target_pairs={{2,0},{4,2},{6,4},{8,6},{10,8},{12,10},{14,12},{16,14},{18,16},{20... | collective-permute-start | bytes 49160 | tf_op jit(solution)/shard_map/ppermute | solution.py:243
  5.7 3.0 %collective-permute-start.1 = (bf16[16,512]{1,0:T(8,128)(2,1)S(1)}, bf16[16,512]{1,0:T(8,128)(2,1)S(1)}, u32[]{:S(2)}, u32[]{:S(2)}) collective-permute-start(bf16[16,512]{1,0:T(8,128)(2,1)S(1)} %get-tuple-element.27), channel_id=1, source_target_pairs={{0,2},{2,4},{4,6},{6,8},{8,10},{10,12},{12,14},{14,16},{16,18},{18... | collective-permute-start | bytes 49160 | tf_op jit(solution)/shard_map/ppermute | solution.py:242
  9.6 3.0 %collective-permute-start.4 = (bf16[2,32,512]{2,1,0:T(8,128)(2,1)S(1)}, bf16[2,32,512]{2,1,0:T(8,128)(2,1)S(1)}, u32[]{:S(2)}, u32[]{:S(2)}) collective-permute-start(bf16[2,32,512]{2,1,0:T(8,128)(2,1)S(1)} %pad_maximum_fusion), channel_id=1, source_target_pairs={{0,2},{2,4},{4,6},{6,8},{8,10},{10,12},{12,14},{14,16},{16,18},{18... | collective-permute-start | bytes 196616 | tf_op jit(solution)/shard_map/ppermute | solution.py:239
  13.3 1.3 %collective-permute-start.5 = (bf16[2,32,512]{2,1,0:T(8,128)(2,1)S(1)}, bf16[2,32,512]{2,1,0:T(8,128)(2,1)S(1)}, u32[]{:S(2)}, u32[]{:S(2)}) collective-permute-start(bf16[2,32,512]{2,1,0:T(8,128)(2,1)S(1)} %pad_maximum_fusion.1), channel_id=1, source_target_pairs={{2,0},{4,2},{6,4},{8,6},{10,8},{12,10},{14,12},{16,14},{18,16},{20... | collective-permute-start | bytes 196616 | tf_op jit(solution)/shard_map/ppermute | solution.py:240
  15.4 12.4 %collective-permute-done.3 = bf16[2,16,512]{2,1,0:T(8,128)(2,1)S(1)} collective-permute-done((bf16[2,16,512]{2,1,0:T(8,128)(2,1)S(1)}, bf16[2,16,512]{2,1,0:T(8,128)(2,1)S(1)}, u32[]{:S(2)}, u32[]{:S(2)}) %collective-permute-start.3) | collective-permute-done | bytes 32800 | tf_op jit(solution)/shard_map/ppermute | solution.py:245
  27.8 1.2 %copy-done.1 = bf16[1024,512]{1,0:T(8,128)(2,1)S(1)} copy-done((bf16[1024,512]{1,0:T(8,128)(2,1)S(1)}, bf16[1024,512]{1,0:T(8,128)(2,1)}, u32[]{:S(2)}) %copy-start.1) | copy-done | bytes 1048600
  29.1 1.2 %copy-done.3 = bf16[1024,512]{1,0:T(8,128)(2,1)S(1)} copy-done((bf16[1024,512]{1,0:T(8,128)(2,1)S(1)}, bf16[1024,512]{1,0:T(8,128)(2,1)}, u32[]{:S(2)}) %copy-start.3) | copy-done | bytes 1048600
  31.0 13.2 %shard_map.101 = (f32[4,1088,128]{2,1,0:T(8,128)}, f32[4,1056,128]{2,1,0:T(8,128)S(1)}, f32[4,1056,128]{2,1,0:T(8,128)}, bf16[1024,512]{1,0:T(8,128)(2,1)S(1)}) custom-call(bf16[1024,512]{1,0:T(8,128)(2,1)S(1)} %copy-done.1, bf16[1024,512]{1,0:T(8,128)(2,1)S(1)} %copy-done.3, bf16[32,512]{1,0:T(8,128)(2,1)S(1)} %get-tuple-element.32.vlo, ...), custom_call_target="tpu_custom_call" | custom-call | flops 32505856 | bytes 10485760 | tf_op jit(solution)/shard_map/pallas_call | solution.py:218
  44.2 1.4 %copy-done.6 = f32[4,1056,128]{2,1,0:T(8,128)} copy-done((f32[4,1056,128]{2,1,0:T(8,128)}, f32[4,1056,128]{2,1,0:T(8,128)S(1)}, u32[]{:S(2)}) %copy-start.6) | copy-done | bytes 2162712
  45.6 10.1 %shard_map.102 = (f32[4,1056,128]{2,1,0:T(8,128)}, f32[8,512]{1,0:T(8,128)S(1)}, f32[1024,512]{1,0:T(8,128)}) custom-call(bf16[1024,512]{1,0:T(8,128)(2,1)S(1)} %copy-done.7, bf16[1,1024,512]{2,1,0:T(8,128)(2,1)S(1)} %bitcast.60, bf16[2,16,512]{2,1,0:T(8,128)(2,1)S(1)} %get-tuple-element.34.elo, bf16[2,16,512]{2,1,0:T(8,128)(2,1)S(1)} %get-tuple-element.33.ehi, ...), custom_call_target="tpu_custom_call" | custom-call | flops 2147483648 | bytes 10485760 | tf_op jit(solution)/shard_map/pallas_call | solution.py:218
  55.7 1.4 %fusion = bf16[8,64,512]{2,1,0:T(8,128)(2,1)S(1)} fusion(f32[8,2,64,512]{3,2,1,0:T(8,128)} %bitcast.69, s32[]{:T(128)S(6)} %select_n.60), kind=kLoop, calls=%fused_computation.2 | loop fusion | bytes 1048580 | tf_op jit(solution)/shard_map/convert_element_type | solution.py:271
  57.3 1.9 %collective-permute-done.10 = bf16[8,64,512]{2,1,0:T(8,128)(2,1)S(1)} collective-permute-done((bf16[8,64,512]{2,1,0:T(8,128)(2,1)S(1)}, bf16[8,64,512]{2,1,0:T(8,128)(2,1)S(1)}, u32[]{:S(2)}, u32[]{:S(2)}) %collective-permute-start.10) | collective-permute-done | bytes 524320 | tf_op jit(solution)/shard_map/ppermute | solution.py:271
  59.1 1.4 %bitcast_add_fusion = f32[8,64,512]{2,1,0:T(8,128)S(1)} fusion(bf16[8,64,512]{2,1,0:T(8,128)(2,1)S(1)} %collective-permute-done.10, f32[8,2,64,512]{3,2,1,0:T(8,128)} %bitcast.70, s32[]{:T(128)S(6)} %select_n.59), kind=kLoop, calls=%fused_computation.1 | loop fusion | flops 524288 | bytes 2621444 | tf_op jit(solution)/shard_map/add | solution.py:271
  61.4 1.7 %collective-permute-start.11 = (bf16[4,64,512]{2,1,0:T(8,128)(2,1)}, bf16[4,64,512]{2,1,0:T(8,128)(2,1)}, u32[]{:S(2)}, u32[]{:S(2)}) collective-permute-start(bf16[4,64,512]{2,1,0:T(8,128)(2,1)} %fusion.1), channel_id=1, source_target_pairs={{0,4},{2,6},{4,0},{6,2},{8,12},{10,14},{12,8},{14,10},{16,20},{18,... | collective-permute-start | bytes 786440 | tf_op jit(solution)/shard_map/ppermute | solution.py:271
  63.1 1.6 %copy-done.5 = f32[4,1088,128]{2,1,0:T(8,128)S(1)} copy-done((f32[4,1088,128]{2,1,0:T(8,128)S(1)}, f32[4,1088,128]{2,1,0:T(8,128)}, u32[]{:S(2)}) %copy-start.5) | copy-done | bytes 2228248
  64.7 7.3 %shard_map.104 = f32[4,32,128]{2,1,0:T(8,128)S(1)} custom-call(f32[4,1056,128]{2,1,0:T(8,128)S(1)} %copy-done, f32[4,1088,128]{2,1,0:T(8,128)S(1)} %copy-done.5, f32[8,512]{1,0:T(8,128)S(1)} %get-tuple-element.21.gain_part), custom_call_target="tpu_custom_call" | custom-call | flops 32505856 | bytes 10485760 | tf_op jit(solution)/shard_map/pallas_call | solution.py:218
  75.7 1.9 %collective-permute-start.12 = (bf16[2,64,512]{2,1,0:T(8,128)(2,1)S(1)}, bf16[2,64,512]{2,1,0:T(8,128)(2,1)}, u32[]{:S(2)}, u32[]{:S(2)}) collective-permute-start(bf16[2,64,512]{2,1,0:T(8,128)(2,1)S(1)} %fusion.2), channel_id=1, source_target_pairs={{0,8},{2,10},{4,12},{6,14},{8,0},{10,2},{12,4},{14,6},{16,24},{18,... | collective-permute-start | bytes 393224 | tf_op jit(solution)/shard_map/ppermute | solution.py:271
  77.7 1.6 %collective-permute-start.8 = (f32[4,32,128]{2,1,0:T(8,128)S(1)}, f32[4,32,128]{2,1,0:T(8,128)S(1)}, u32[]{:S(2)}, u32[]{:S(2)}) collective-permute-start(f32[4,32,128]{2,1,0:T(8,128)S(1)} %add.74), channel_id=1, source_target_pairs={{0,8},{2,10},{4,12},{6,14},{8,0},{10,2},{12,4},{14,6},{16,24},{18,... | collective-permute-start | bytes 196616 | tf_op jit(solution)/shard_map/ppermute | solution.py:272
  79.3 1.2 %copy-done.4 = bf16[1024,512]{1,0:T(8,128)(2,1)S(1)} copy-done((bf16[1024,512]{1,0:T(8,128)(2,1)S(1)}, bf16[1024,512]{1,0:T(8,128)(2,1)}, u32[]{:S(2)}) %copy-start.4) | copy-done | bytes 1048600
  80.5 7.9 %shard_map.103 = (bf16[1024,512]{1,0:T(8,128)(2,1)}, bf16[1024,512]{1,0:T(8,128)(2,1)}) custom-call(f32[4,1056,128]{2,1,0:T(8,128)S(1)} %copy-done, bf16[1024,512]{1,0:T(8,128)(2,1)S(1)} %copy-done.2, bf16[1024,512]{1,0:T(8,128)(2,1)S(1)} %copy-done.4, f32[4,31,128]{2,1,0:T(8,128)S(1)} %bitcast.62), custom_call_target="tpu_custom_call" | custom-call | flops 32505856 | bytes 10485760 | tf_op jit(solution)/shard_map/pallas_call | solution.py:218
  88.4 2.7 %collective-permute-start.9 = (f32[4,32,128]{2,1,0:T(8,128)S(1)}, f32[4,32,128]{2,1,0:T(8,128)S(1)}, u32[]{:S(2)}, u32[]{:S(2)}) collective-permute-start(f32[4,32,128]{2,1,0:T(8,128)S(1)} %add.75), channel_id=1, source_target_pairs={{0,16},{2,18},{4,20},{6,22},{8,24},{10,26},{12,28},{14,30},{16,0},... | collective-permute-start | bytes 196616 | tf_op jit(solution)/shard_map/ppermute | solution.py:272
  92.5 2.0 %collective-permute-done.9 = f32[4,32,128]{2,1,0:T(8,128)S(1)} collective-permute-done((f32[4,32,128]{2,1,0:T(8,128)S(1)}, f32[4,32,128]{2,1,0:T(8,128)S(1)}, u32[]{:S(2)}, u32[]{:S(2)}) %collective-permute-start.9) | collective-permute-done | bytes 65568 | tf_op jit(solution)/shard_map/ppermute | solution.py:272
  95.7 2.1 %collective-permute-done.13 = bf16[1,64,512]{2,1,0:T(8,128)(2,1)S(1)} collective-permute-done((bf16[1,64,512]{2,1,0:T(8,128)(2,1)S(1)}, bf16[1,64,512]{2,1,0:T(8,128)(2,1)S(1)}, u32[]{:S(2)}, u32[]{:S(2)}) %collective-permute-start.13) | collective-permute-done | bytes 65568 | tf_op jit(solution)/shard_map/ppermute | solution.py:271
  (60 shorter events, 11.7 us)
Async XLA Ops:
  0.6 45.0 %copy-start.7 = (bf16[1024,512]{1,0:T(8,128)(2,1)S(1)}, bf16[1024,512]{1,0:T(8,128)(2,1)}, u32[]{:S(2)}) copy-start(bf16[1024,512]{1,0:T(8,128)(2,1)} %grad.1) | copy-start | bytes 3145732
  0.6 44.9 %collective-permute-start = (bf16[1024,512]{1,0:T(8,128)(2,1)}, bf16[1024,512]{1,0:T(8,128)(2,1)S(1)}, u32[]{:S(2)}, u32[]{:S(2)}) collective-permute-start(bf16[1024,512]{1,0:T(8,128)(2,1)} %grad.1), channel_id=1, source_target_pairs={{1,0},{0,1},{3,2},{2,3},{5,4},{4,5},{7,6},{6,7},{9,8},{8,9},{11,10... | collective-permute-start | bytes 3145736 | tf_op jit(solution)/shard_map/ppermute | solution.py:246
  4.5 8.2 %collective-permute-start.2 = (bf16[16,512]{1,0:T(8,128)(2,1)S(1)}, bf16[16,512]{1,0:T(8,128)(2,1)S(1)}, u32[]{:S(2)}, u32[]{:S(2)}) collective-permute-start(bf16[16,512]{1,0:T(8,128)(2,1)S(1)} %get-tuple-element.28), channel_id=1, source_target_pairs={{2,0},{4,2},{6,4},{8,6},{10,8},{12,10},{14,12},{16,14},{18,16},{20... | collective-permute-start | bytes 49160 | tf_op jit(solution)/shard_map/ppermute | solution.py:243
  5.7 6.9 %collective-permute-start.1 = (bf16[16,512]{1,0:T(8,128)(2,1)S(1)}, bf16[16,512]{1,0:T(8,128)(2,1)S(1)}, u32[]{:S(2)}, u32[]{:S(2)}) collective-permute-start(bf16[16,512]{1,0:T(8,128)(2,1)S(1)} %get-tuple-element.27), channel_id=1, source_target_pairs={{0,2},{2,4},{4,6},{6,8},{8,10},{10,12},{12,14},{14,16},{16,18},{18... | collective-permute-start | bytes 49160 | tf_op jit(solution)/shard_map/ppermute | solution.py:242
  9.6 18.2 %collective-permute-start.4 = (bf16[2,32,512]{2,1,0:T(8,128)(2,1)S(1)}, bf16[2,32,512]{2,1,0:T(8,128)(2,1)S(1)}, u32[]{:S(2)}, u32[]{:S(2)}) collective-permute-start(bf16[2,32,512]{2,1,0:T(8,128)(2,1)S(1)} %pad_maximum_fusion), channel_id=1, source_target_pairs={{0,2},{2,4},{4,6},{6,8},{8,10},{10,12},{12,14},{14,16},{16,18},{18... | collective-permute-start | bytes 196616 | tf_op jit(solution)/shard_map/ppermute | solution.py:239
  12.7 15.1 %collective-permute-start.3 = (bf16[2,16,512]{2,1,0:T(8,128)(2,1)S(1)}, bf16[2,16,512]{2,1,0:T(8,128)(2,1)S(1)}, u32[]{:S(2)}, u32[]{:S(2)}) collective-permute-start(bf16[2,16,512]{2,1,0:T(8,128)(2,1)S(1)} %get-tuple-element.35), channel_id=1, source_target_pairs={{1,0},{0,1},{3,2},{2,3},{5,4},{4,5},{7,6},{6,7},{9,8},{8,9},{11,10... | collective-permute-start | bytes 98312 | tf_op jit(solution)/shard_map/ppermute | solution.py:245
  13.3 14.5 %collective-permute-start.5 = (bf16[2,32,512]{2,1,0:T(8,128)(2,1)S(1)}, bf16[2,32,512]{2,1,0:T(8,128)(2,1)S(1)}, u32[]{:S(2)}, u32[]{:S(2)}) collective-permute-start(bf16[2,32,512]{2,1,0:T(8,128)(2,1)S(1)} %pad_maximum_fusion.1), channel_id=1, source_target_pairs={{2,0},{4,2},{6,4},{8,6},{10,8},{12,10},{14,12},{16,14},{18,16},{20... | collective-permute-start | bytes 196616 | tf_op jit(solution)/shard_map/ppermute | solution.py:240
  27.8 1.2 %copy-start.1 = (bf16[1024,512]{1,0:T(8,128)(2,1)S(1)}, bf16[1024,512]{1,0:T(8,128)(2,1)}, u32[]{:S(2)}) copy-start(bf16[1024,512]{1,0:T(8,128)(2,1)} %value.3) | copy-start | bytes 3145732
  31.0 14.6 %copy-start.8 = (bf16[1024,512]{1,0:T(8,128)(2,1)S(1)}, bf16[1024,512]{1,0:T(8,128)(2,1)}, u32[]{:S(2)}) copy-start(bf16[1024,512]{1,0:T(8,128)(2,1)} %weight.1) | copy-start | bytes 3145732
  44.2 1.4 %copy-start.6 = (f32[4,1056,128]{2,1,0:T(8,128)}, f32[4,1056,128]{2,1,0:T(8,128)S(1)}, u32[]{:S(2)}) copy-start(f32[4,1056,128]{2,1,0:T(8,128)S(1)} %get-tuple-element.14.unit) | copy-start | bytes 6488068
  55.7 7.4 %copy-start = (f32[4,1056,128]{2,1,0:T(8,128)S(1)}, f32[4,1056,128]{2,1,0:T(8,128)}, u32[]{:S(2)}) copy-start(f32[4,1056,128]{2,1,0:T(8,128)} %get-tuple-element.17.dconv) | copy-start | bytes 6488068
  57.1 2.0 %collective-permute-start.10 = (bf16[8,64,512]{2,1,0:T(8,128)(2,1)S(1)}, bf16[8,64,512]{2,1,0:T(8,128)(2,1)S(1)}, u32[]{:S(2)}, u32[]{:S(2)}) collective-permute-start(bf16[8,64,512]{2,1,0:T(8,128)(2,1)S(1)} %fusion), channel_id=1, source_target_pairs={{0,2},{2,0},{4,6},{6,4},{8,10},{10,8},{12,14},{14,12},{16,18},{18,... | collective-permute-start | bytes 1572872 | tf_op jit(solution)/shard_map/ppermute | solution.py:271
  60.5 2.5 %copy-start.10 = (f32[8,64,512]{2,1,0:T(8,128)}, f32[8,64,512]{2,1,0:T(8,128)S(1)}, u32[]{:S(2)}) copy-start(f32[8,64,512]{2,1,0:T(8,128)S(1)} %bitcast_add_fusion) | copy-start | bytes 3145732
  61.4 12.3 %collective-permute-start.11 = (bf16[4,64,512]{2,1,0:T(8,128)(2,1)}, bf16[4,64,512]{2,1,0:T(8,128)(2,1)}, u32[]{:S(2)}, u32[]{:S(2)}) collective-permute-start(bf16[4,64,512]{2,1,0:T(8,128)(2,1)} %fusion.1), channel_id=1, source_target_pairs={{0,4},{2,6},{4,0},{6,2},{8,12},{10,14},{12,8},{14,10},{16,20},{18,... | collective-permute-start | bytes 786440 | tf_op jit(solution)/shard_map/ppermute | solution.py:271
  63.1 1.6 %copy-start.5 = (f32[4,1088,128]{2,1,0:T(8,128)S(1)}, f32[4,1088,128]{2,1,0:T(8,128)}, u32[]{:S(2)}) copy-start(f32[4,1088,128]{2,1,0:T(8,128)} %get-tuple-element.20.gated) | copy-start | bytes 6684676
  64.7 14.6 %copy-start.2 = (bf16[1024,512]{1,0:T(8,128)(2,1)S(1)}, bf16[1024,512]{1,0:T(8,128)(2,1)}, u32[]{:S(2)}) copy-start(bf16[1024,512]{1,0:T(8,128)(2,1)} %value.3) | copy-start | bytes 3145732
  72.0 1.3 %collective-permute-start.6 = (f32[4,32,128]{2,1,0:T(8,128)S(1)}, f32[4,32,128]{2,1,0:T(8,128)S(1)}, u32[]{:S(2)}, u32[]{:S(2)}) collective-permute-start(f32[4,32,128]{2,1,0:T(8,128)S(1)} %shard_map.104), channel_id=1, source_target_pairs={{0,2},{2,0},{4,6},{6,4},{8,10},{10,8},{12,14},{14,12},{16,18},{18,... | collective-permute-start | bytes 196616 | tf_op jit(solution)/shard_map/ppermute | solution.py:272
  73.3 4.3 %collective-permute-start.7 = (f32[4,32,128]{2,1,0:T(8,128)S(1)}, f32[4,32,128]{2,1,0:T(8,128)S(1)}, u32[]{:S(2)}, u32[]{:S(2)}) collective-permute-start(f32[4,32,128]{2,1,0:T(8,128)S(1)} %add.73), channel_id=1, source_target_pairs={{0,4},{2,6},{4,0},{6,2},{8,12},{10,14},{12,8},{14,10},{16,20},{18,... | collective-permute-start | bytes 196616 | tf_op jit(solution)/shard_map/ppermute | solution.py:272
  75.7 15.4 %collective-permute-start.12 = (bf16[2,64,512]{2,1,0:T(8,128)(2,1)S(1)}, bf16[2,64,512]{2,1,0:T(8,128)(2,1)}, u32[]{:S(2)}, u32[]{:S(2)}) collective-permute-start(bf16[2,64,512]{2,1,0:T(8,128)(2,1)S(1)} %fusion.2), channel_id=1, source_target_pairs={{0,8},{2,10},{4,12},{6,14},{8,0},{10,2},{12,4},{14,6},{16,24},{18,... | collective-permute-start | bytes 393224 | tf_op jit(solution)/shard_map/ppermute | solution.py:271
  77.7 10.8 %collective-permute-start.8 = (f32[4,32,128]{2,1,0:T(8,128)S(1)}, f32[4,32,128]{2,1,0:T(8,128)S(1)}, u32[]{:S(2)}, u32[]{:S(2)}) collective-permute-start(f32[4,32,128]{2,1,0:T(8,128)S(1)} %add.74), channel_id=1, source_target_pairs={{0,8},{2,10},{4,12},{6,14},{8,0},{10,2},{12,4},{14,6},{16,24},{18,... | collective-permute-start | bytes 196616 | tf_op jit(solution)/shard_map/ppermute | solution.py:272
  79.3 1.2 %copy-start.4 = (bf16[1024,512]{1,0:T(8,128)(2,1)S(1)}, bf16[1024,512]{1,0:T(8,128)(2,1)}, u32[]{:S(2)}) copy-start(bf16[1024,512]{1,0:T(8,128)(2,1)} %gate.3) | copy-start | bytes 3145732
  80.5 10.6 %copy-start.12 = (f32[4,64,512]{2,1,0:T(8,128)S(1)}, f32[4,64,512]{2,1,0:T(8,128)}, u32[]{:S(2)}) copy-start(f32[4,64,512]{2,1,0:T(8,128)} %copy-done.11) | copy-start | bytes 1572868
  88.4 6.0 %collective-permute-start.9 = (f32[4,32,128]{2,1,0:T(8,128)S(1)}, f32[4,32,128]{2,1,0:T(8,128)S(1)}, u32[]{:S(2)}, u32[]{:S(2)}) collective-permute-start(f32[4,32,128]{2,1,0:T(8,128)S(1)} %add.75), channel_id=1, source_target_pairs={{0,16},{2,18},{4,20},{6,22},{8,24},{10,26},{12,28},{14,30},{16,0},... | collective-permute-start | bytes 196616 | tf_op jit(solution)/shard_map/ppermute | solution.py:272
  92.1 5.8 %collective-permute-start.13 = (bf16[1,64,512]{2,1,0:T(8,128)(2,1)S(1)}, bf16[1,64,512]{2,1,0:T(8,128)(2,1)S(1)}, u32[]{:S(2)}, u32[]{:S(2)}) collective-permute-start(bf16[1,64,512]{2,1,0:T(8,128)(2,1)S(1)} %dynamic-slice_convert_fusion.2), channel_id=1, source_target_pairs={{0,16},{2,18},{4,20},{6,22},{8,24},{10,26},{12,28},{14,30},{16,0},... | collective-permute-start | bytes 196616 | tf_op jit(solution)/shard_map/ppermute | solution.py:271
  (3 other events, 2.7 us)

commit v2 on v0

v2 whole, which is shorter than its diff:
```python
import functools

import jax
import jax.numpy as jnp
from jax import lax
from jax.experimental import pallas as pl
from jax.experimental.pallas import tpu as pltpu
from jax.sharding import PartitionSpec as P

GROUP = 64
EPS = 1e-06
LANE = 128
EDGE = 16
F32, BF16 = jnp.float32, jnp.bfloat16


def sigmoid(x):
    return 0.5 * jnp.tanh(0.5 * x) + 0.5


def divisor(total, *choices):
    for choice in choices:
        if total % choice == 0:
            return choice
    return total


def group_matrix():
    row = lax.broadcasted_iota(jnp.int32, (2 * LANE, LANE), 0)
    col = lax.broadcasted_iota(jnp.int32, (2 * LANE, LANE), 1)
    same = lax.rem(row, LANE) // GROUP == col // GROUP
    return jnp.where(same, 1.0 / GROUP, 0.0).astype(BF16)


def group_mean(x, matrix):
    high = x.astype(BF16)
    low = (x - high.astype(F32)).astype(BF16)
    return jnp.dot(jnp.concatenate([high, low], axis=1), matrix, preferred_element_type=F32)


def lanes(c):
    return pl.ds(pl.multiple_of(c * LANE, LANE), LANE)


def put_gated(gated, c, v, g, dst, n):
    gated[c, pl.ds(dst, n), :] = (v.astype(F32) * sigmoid(g.astype(F32))).astype(BF16).astype(F32)


def forward_tile(c, taps, gain, gated, unit, inv, normed, matrix):
    kw = taps.shape[1]
    extent = unit.shape[1]
    rows = normed.shape[0]
    cstep = divisor(extent, 96, 32)

    def conv(r, _):
        at = r * cstep
        acc = jnp.zeros((cstep, LANE), F32)
        for k in range(kw):
            acc += taps[c, pl.ds(k, 1), :] * gated[c, pl.ds(at + (k + EDGE - kw // 2), cstep), :]
        unit[c, pl.ds(pl.multiple_of(at, 8), cstep), :] = acc
        return 0

    lax.fori_loop(0, extent // cstep, conv, 0)
    nstep = divisor(extent, 352, 32)

    def norm(r, _):
        at = pl.multiple_of(r * nstep, 8)
        x = unit[c, pl.ds(at, nstep), :]
        centred = x - group_mean(x, matrix)
        rs = lax.rsqrt(group_mean(centred * centred, matrix) + EPS)
        inv[c, pl.ds(at, nstep), :] = rs
        unit[c, pl.ds(at, nstep), :] = centred * rs
        return 0

    lax.fori_loop(0, extent // nstep, norm, 0)
    step = divisor(rows, 256, 32)

    def act(r, _):
        at = pl.multiple_of(r * step, step)
        p = unit[c, pl.ds(pl.multiple_of(at + EDGE, 8), step), :] * gain[:, lanes(c)]
        normed[pl.ds(at, step), lanes(c)] = (p * sigmoid(p)).astype(BF16)
        return 0

    lax.fori_loop(0, rows // step, act, 0)


def act_to_conv(ng, at, n, own, unit, inv, gain, dconv, gain_part, matrix):
    for c in range(unit.shape[0]):
        g = gain[:, c * LANE:(c + 1) * LANE]
        u = unit[c, pl.ds(at, n), :]
        p = u * g
        s = sigmoid(p)
        a = ng[:, c * LANE:(c + 1) * LANE] * s * (1.0 + p * (1.0 - s))
        au = a * u
        if own:
            gain_part[:, c * LANE:(c + 1) * LANE] += jnp.sum(au.reshape(n // 8, 8, LANE), axis=0)
        h = a * g
        hu = au * g
        dconv[c, pl.ds(at, n), :] = inv[c, pl.ds(at, n), :] * (
            h - group_mean(h, matrix) - u * group_mean(hu, matrix))


def taps_tile(c, dconv, gated, gain_part, sums):
    kw = sums.shape[1] - 1
    rows = dconv.shape[1] - 2 * EDGE

    def chunk(r, accs):
        at = r * 16
        out = []
        d0 = dconv[c, pl.ds(pl.multiple_of(at + EDGE, 8), 8), :]
        d1 = dconv[c, pl.ds(pl.multiple_of(at + EDGE + 8, 8), 8), :]
        for k in range(kw):
            g0 = gated[c, pl.ds(at + (k + 2 * EDGE - kw // 2), 8), :]
            g1 = gated[c, pl.ds(at + (k + 2 * EDGE - kw // 2 + 8), 8), :]
            out.append(accs[k] + (d0 * g0 + d1 * g1))
        return tuple(out)

    accs = lax.fori_loop(0, rows // 16, chunk, tuple(jnp.zeros((8, LANE), F32) for _ in range(kw)))
    for k in range(kw):
        sums[c, pl.ds(k, 1), :] = jnp.sum(accs[k], axis=0, keepdims=True)
    sums[c, pl.ds(kw, 1), :] = jnp.sum(gain_part[:, lanes(c)], axis=0, keepdims=True)


def backward_tile(c, dconv, value, gate, taps, vgrad, ggrad):
    rows = value.shape[0]
    kw = taps.shape[1]
    step = divisor(rows, 64, 32)

    def chunk(r, _):
        at = pl.multiple_of(r * step, step)
        acc = jnp.zeros((step, LANE), F32)
        for k in range(kw):
            acc += taps[c, pl.ds(k, 1), :] * dconv[c, pl.ds(at + (EDGE + kw // 2 - k), step), :]
        s = sigmoid(gate[pl.ds(at, step), lanes(c)].astype(F32))
        v = value[pl.ds(at, step), lanes(c)].astype(F32)
        gs = acc * s
        vgrad[pl.ds(at, step), lanes(c)] = gs.astype(BF16)
        ggrad[pl.ds(at, step), lanes(c)] = (gs * v * (1.0 - s)).astype(BF16)
        return 0

    lax.fori_loop(0, rows // step, chunk, 0)


def loop(lo, hi, body):
    def one(i, _):
        body(i)
        return 0

    lax.fori_loop(lo, hi, one, 0)


def whole_kernel(n, peers, value, gate, taps, gain, weight, grad,
                 vgrad, ggrad, out_sums, wout,
                 gated, unit, inv, normed, dconv, gain_part, wpart, sums,
                 vhalo, ohalo, others, send1, recv1, send2, recv2, send3, recv3,
                 arecv1, arecv2, asum, arecv3, atotal,
                 vs, vr, os_, or_, gs, gr, ws, wr, ws3, wr3, as_, ar, as3, ar3):
    rows, chans = value.shape
    tiles = chans // LANE
    sp, tp = lax.axis_index("sp"), lax.axis_index("tp")
    group = recv3.shape[0] + 1
    half_tiles = tiles // 2
    b0, b1, zz = lax.rem(sp, 2), lax.rem(sp // 2, 2), sp // 4
    left, right = lax.rem(sp + n - 1, n), lax.rem(sp + 1, n)
    mate0 = sp + 1 - 2 * b0
    mate1 = sp + 2 - 4 * b1

    def zmate(d):
        return lax.rem(sp + 4 * d, n)

    def tmate(j):
        return lax.rem(tp + peers - j, peers)

    def remote(src, dst, s, r, to):
        return pltpu.make_async_remote_copy(
            src_ref=src, dst_ref=dst, send_sem=s, recv_sem=r, device_id=to,
            device_id_type=pl.DeviceIdType.MESH)

    barrier = pltpu.get_barrier_semaphore()
    friends = [(left, tmate(j)) for j in range(peers)] + [(right, tmate(j)) for j in range(peers)]
    friends += [(sp, tmate(j)) for j in range(1, peers)] + [(mate0, tp), (mate1, tp)]
    friends += [(zmate(d), tp) for d in range(1, group)]
    for friend in friends:
        pl.semaphore_signal(barrier, inc=1, device_id=friend, device_id_type=pl.DeviceIdType.MESH)
    pl.semaphore_wait(barrier, len(friends))

    wide = 2 * EDGE
    pending = []
    halos = []
    for side, (start, to) in enumerate(((rows - wide, right), (0, left))):
        for i, ref in enumerate((value, gate)):
            halos.append(remote(ref.at[pl.ds(start, wide)], vhalo.at[side, i], vs.at[side, i], vr.at[side, i], (to, tp)))
    ohalos = []
    for side, (start, to) in enumerate(((rows - EDGE, right), (0, left))):
        for j in range(peers):
            ohalos.append(remote(grad.at[pl.ds(start, EDGE)], ohalo.at[side, j], os_.at[side, j], or_.at[side, j], (to, tmate(j))))
    for copy in halos + ohalos:
        copy.start()
    pending += halos + ohalos
    chunks = gs.shape[1]
    step = rows // chunks

    def gather(j, r):
        at = pl.ds(pl.multiple_of(r * step, step), step)
        return remote(grad.at[at], others.at[j - 1, at], gs.at[j - 1, r], gr.at[j - 1, r], (sp, tmate(j)))

    for r in range(chunks):
        for j in range(1, peers):
            copy = gather(j, r)
            copy.start()
            pending.append(copy)

    matrix = group_matrix()
    gstep = divisor(rows, 256, 32)

    def own_gated(c):
        def chunk(r):
            at = pl.multiple_of(r * gstep, gstep)
            put_gated(gated, c, value[pl.ds(at, gstep), lanes(c)], gate[pl.ds(at, gstep), lanes(c)],
                      pl.multiple_of(at + wide, 8), gstep)

        loop(0, rows // gstep, chunk)

    loop(0, tiles, own_gated)
    for copy in halos:
        copy.wait_recv()
    inside = ((sp > 0).astype(F32), (sp < n - 1).astype(F32))

    def front(c):
        for side, dst in ((0, 0), (1, rows + wide)):
            put_gated(gated, c, vhalo[side, 0, :, lanes(c)].astype(F32) * inside[side],
                      vhalo[side, 1, :, lanes(c)], dst, wide)
        forward_tile(c, taps, gain, gated, unit, inv, normed, matrix)

    loop(0, tiles, front)

    def owner(j):
        return pl.ds(pl.multiple_of(lax.rem(tp + j, peers) * chans, chans), chans)

    per = wpart.shape[1]
    piece = max(divisor(chans, 256, 128), per)

    def weight_part(j):
        def cols(q):
            at = pl.ds(pl.multiple_of(q * piece, piece), piece)
            lhs = grad[:, at] if j == 0 else others[j - 1, :, at]
            out = lax.dot_general(lhs, normed[...], (((0,), (0,)), ((), ())), preferred_element_type=F32)
            base = lax.rem(tp + j, peers) * (chans // per) + q * (piece // per)
            wpart[pl.ds(base, piece // per)] = out.reshape(piece // per, per, chans)

        loop(0, chans // piece, cols)

    weight_part(0)
    gain_part[...] = jnp.zeros_like(gain_part)
    for copy in ohalos:
        copy.wait_recv()
    for side, at in ((0, 0), (1, rows + EDGE)):
        ng = sum(jnp.dot(ohalo[side, j], weight[owner(j), :], preferred_element_type=F32) for j in range(peers))
        act_to_conv(ng * inside[side], at, EDGE, False, unit, inv, gain, dconv, gain_part, matrix)

    def middle(r):
        at = pl.multiple_of(r * step, step)
        ng = jnp.dot(grad[pl.ds(at, step), :], weight[owner(0), :], preferred_element_type=F32)
        for j in range(1, peers):
            gather(j, r).wait_recv()
            ng += jnp.dot(others[j - 1, pl.ds(at, step), :], weight[owner(j), :], preferred_element_type=F32)
        act_to_conv(ng, pl.multiple_of(at + EDGE, 8), step, True, unit, inv, gain, dconv, gain_part, matrix)

    loop(0, chunks, middle)
    for j in range(1, peers):
        weight_part(j)

    def cast1(a):
        send1[a] = wpart[2 * a + 1 - b0].astype(BF16)

    loop(0, n // 2, cast1)
    copy1 = remote(send1, recv1, ws.at[0], wr.at[0], (mate0, tp))
    copy1.start()
    loop(0, half_tiles, lambda c: taps_tile(c, dconv, gated, gain_part, sums))
    copy1.wait_recv()

    def cast2(a):
        other, mine = 2 * a + 1 - b1, 2 * a + b1
        send2[a] = (wpart[2 * other + b0] + recv1[other].astype(F32)).astype(BF16)
        wpart[2 * mine + b0] = wpart[2 * mine + b0] + recv1[mine].astype(F32)

    loop(0, n // 4, cast2)
    copy2 = remote(send2, recv2, ws.at[1], wr.at[1], (mate1, tp))
    copy2.start()
    loop(half_tiles, tiles, lambda c: taps_tile(c, dconv, gated, gain_part, sums))

    acopy1 = remote(sums.at[pl.ds((1 - b0) * half_tiles, half_tiles)], arecv1, as_.at[0], ar.at[0], (mate0, tp))
    acopy1.start()
    quarter = max(tiles // 4, 1)
    loop(0, quarter, lambda c: backward_tile(c, dconv, value, gate, taps, vgrad, ggrad))
    acopy1.wait_recv()
    asum[0] = sums[pl.ds(b0 * half_tiles, half_tiles)] + arecv1[...]
    acopy2 = remote(asum.at[0], arecv2, as_.at[1], ar.at[1], (mate1, tp))
    acopy2.start()
    copy2.wait_recv()

    def total2(z):
        return wpart[4 * z + 2 * b1 + b0] + recv2[z].astype(F32)

    copies3 = []
    for d in range(1, group):
        send3[d - 1] = total2(lax.rem(zz + d, group)).astype(BF16)
    for d in range(1, group):
        copy = remote(send3.at[d - 1], recv3.at[d - 1], ws3.at[d - 1], wr3.at[d - 1], (zmate(d), tp))
        copy.start()
        copies3.append(copy)
    loop(quarter, 2 * quarter, lambda c: backward_tile(c, dconv, value, gate, taps, vgrad, ggrad))
    acopy2.wait_recv()
    asum[1] = asum[0] + arecv2[...]
    acopies3 = []
    for d in range(1, group):
        copy = remote(asum.at[1], arecv3.at[zz], as3.at[d - 1], ar3.at[d - 1], (zmate(d), tp))
        copy.start()
        acopies3.append(copy)
    loop(2 * quarter, tiles, lambda c: backward_tile(c, dconv, value, gate, taps, vgrad, ggrad))
    for d in range(1, group):
        peer = lax.rem(zz + group - d, group)
        remote(asum.at[1], arecv3.at[peer], as3.at[d - 1], ar3.at[d - 1], (zmate(d), tp)).wait_recv()
    arecv3[zz] = asum[1]
    total = arecv3[0]
    for z in range(1, group):
        total += arecv3[z]
    atotal[b0] = total
    acopy4 = remote(atotal.at[b0], atotal.at[b0], as_.at[2], ar.at[2], (mate0, tp))
    acopy4.start()
    final = total2(zz)
    for d in range(1, group):
        copies3[d - 1].wait_recv()
        final += recv3[d - 1].astype(F32)
    wout[...] = final
    remote(atotal.at[1 - b0], atotal.at[1 - b0], as_.at[2], ar.at[2], (mate0, tp)).wait_recv()
    out_sums[...] = atotal[...].reshape(out_sums.shape)
    for copy in pending + [copy1, copy2, acopy1, acopy2, acopy4] + copies3 + acopies3:
        copy.wait_send()


def per_device(value, gate, conv_taps, norm_gain, point_weight, out_grad):
    rows, chans = value.shape
    kw = conv_taps.shape[0]
    tiles = chans // LANE
    n, peers = lax.axis_size("sp"), lax.axis_size("tp")
    extent = rows + 2 * EDGE
    full = point_weight.shape[0]
    per = full // n
    group = n // 4
    taps = conv_taps.astype(F32).reshape(kw, tiles, LANE).transpose(1, 0, 2)
    gain = norm_gain.reshape(1, chans)
    args = (value, gate, taps, gain, point_weight, out_grad)
    half = (tiles // 2, kw + 1, LANE)
    vmem, dma = pltpu.VMEM, pltpu.SemaphoreType.DMA
    chunks = 4
    outs = [((rows, chans), BF16), ((rows, chans), BF16), ((tiles, kw + 1, LANE), F32), ((per, chans), F32)]
    vgrad, ggrad, sums, wgrad = pl.pallas_call(
        functools.partial(whole_kernel, n, peers),
        out_shape=[jax.ShapeDtypeStruct(s, d) for s, d in outs],
        in_specs=[pl.BlockSpec(memory_space=pltpu.VMEM)] * len(args),
        out_specs=[pl.BlockSpec(memory_space=pltpu.VMEM)] * len(outs),
        scratch_shapes=[
            vmem((tiles, rows + 4 * EDGE, LANE), F32),
            vmem((tiles, extent, LANE), F32),
            vmem((tiles, extent, LANE), F32),
            vmem((rows, chans), BF16),
            vmem((tiles, extent, LANE), F32),
            vmem((8, chans), F32),
            vmem((n, per, chans), F32),
            vmem((tiles, kw + 1, LANE), F32),
            vmem((2, 2, 2 * EDGE, chans), BF16),
            vmem((2, peers, EDGE, chans), BF16),
            vmem((peers - 1, rows, chans), BF16),
            vmem((n // 2, per, chans), BF16),
            vmem((n // 2, per, chans), BF16),
            vmem((n // 4, per, chans), BF16),
            vmem((n // 4, per, chans), BF16),
            vmem((group - 1, per, chans), BF16),
            vmem((group - 1, per, chans), BF16),
            vmem(half, F32),
            vmem(half, F32),
            vmem((2,) + half, F32),
            vmem((group,) + half, F32),
            vmem((2,) + half, F32),
            dma((2, 2)), dma((2, 2)), dma((2, peers)), dma((2, peers)),
            dma((peers - 1, chunks)), dma((peers - 1, chunks)),
            dma((2,)), dma((2,)), dma((group - 1,)), dma((group - 1,)),
            dma((3,)), dma((3,)), dma((group - 1,)), dma((group - 1,)),
        ],
        compiler_params=pltpu.CompilerParams(
            collective_id=0, has_side_effects=True, vmem_limit_bytes=56 * 1024 * 1024),
    )(*args)
    flat = sums.transpose(1, 0, 2).reshape(kw + 1, chans)
    return vgrad, ggrad, flat[:kw], flat[kw], wgrad


def solution(mesh):
    return jax.shard_map(
        per_device,
        mesh=mesh,
        in_specs=(P("sp", "tp"), P("sp", "tp"), P(None, "tp"), P("tp"), P(None, "tp"), P("sp", "tp")),
        out_specs=(P("sp", "tp"), P("sp", "tp"), P(None, "tp"), P("tp"), P("sp", "tp")),
        check_vma=False,
    )
```

time: 249 us -> 66.6 us (0.27)
  waiting for transfers between devices: 126 us -> 0 us
  other arithmetic: 58 us -> 0 us
  Pallas kernels: 0 us -> 57.3 us
  local copies, waits for them, and re-layouts: 29.5 us -> 8.28 us
  between operations: 14.2 us -> 0.66 us
  matrix products: 12.9 us -> 0 us
  starting transfers between devices: 7.56 us -> 0 us
    unnamed x4 -> x0, waiting for transfers between devices: 68.4 us -> none
    pallas_call x0 -> x1, Pallas kernels: none -> 57.3 us  [per_device(): pl.pallas_call(functools.partial(whole_kernel, n, peers), out_shape=[jax....]
    psum x1 -> x0, waiting for transfers between devices: 49.6 us -> none  [per_device(): taps_grad, gain_grad = lax.psum((taps_part, gain_part), 'sp')]
    convert_element_type x3 -> x0, other arithmetic: 21.3 us -> none  [the longest x1 15.9 us: per_device(): (gated_grad * value_f * gate_sig * (1.0 - gate_sig)).astype(jnp.bfloat16)]
    reduce_sum x8 -> x0, other arithmetic: 20.8 us -> none  [the longest x5 16.1 us: per_device(): jnp.sum(conv_grad * gated_wide[margin + tap_index:margin + tap_index + ro...]
    add x1 -> x0, other arithmetic: 14 us -> none  [per_device(): convolved + taps_f[tap_index] * gated_wide[tap_index:tap_index + extent]....]
    dot_general x2 -> x0, matrix products: 12.9 us -> none  [the longest x1 7.9 us: per_device(): jnp.dot(full_grad, point_weight, preferred_element_type=jnp.float32)]
    ppermute x4 -> x0, starting transfers between devices: 7.44 us -> none  [the longest x2 4.86 us: extended(): before = lax.ppermute(last, axis, up)]
  transfers between devices with their start and end apart: 7 -> 0, of which waited for: 5 -> 0; matrix products, arithmetic and copies ran while one was open for 24% -> 0% of each run, Pallas kernels for 0% -> 0%
where the time goes in v2:
time: 66.6 us; the launch traced here: 66.3 us
  Pallas kernels  57.3 us (86%)
  local copies, waits for them, and re-layouts  8.28 us (12%)
    pallas_call x1, Pallas kernels, per_device(): pl.pallas_call(functools.partial(whole_kernel, n, peers), out_shape=[jax....  57.3 us
    unnamed x9, local copies, waits for them, and re-layouts  4.68 us
    slice x2, local copies, waits for them, and re-layouts, per_device(): return (vgrad, ggrad, flat[:kw], flat[kw], wgrad)  2.18 us
    transpose x2, local copies, waits for them, and re-layouts, per_device(): taps = conv_taps.astype(F32).reshape(kw, tiles, LANE).transpose(1, 0, 2)  1.42 us

profile of v2, /device:TPU:0, one launch (start us, length us, event | category | flops | bytes accessed | tf_op | source)
XLA Modules:
  0.0 66.3 jit_solution(5354044657519303835)
XLA Ops:
  0.6 0.8 %reshape.23 = f32[31,4,128]{2,1,0:T(4,128)S(1)} reshape(bf16[31,512]{1,0:T(8,128)(2,1)} %param.8) | data formatting | bytes 95232 | tf_op jit(solution)/shard_map/transpose | solution.py:351
  1.4 0.6 copy.15
  2.1 57.3 %shard_map.101 = (bf16[1024,512]{1,0:T(8,128)(2,1)}, bf16[1024,512]{1,0:T(8,128)(2,1)}, f32[4,32,128]{2,1,0:T(8,128)}, f32[64,512]{1,0:T(8,128)}) custom-call(bf16[1024,512]{1,0:T(8,128)(2,1)} %value.1, bf16[1024,512]{1,0:T(8,128)(2,1)} %gate.1, f32[4,31,128]{2,1,0:T(8,128)} %bitcast.10, f32[1,512]{1,0:T(1,128)} %bitcast.15, bf16[1024,512]{1,0:T(8,128)(2,1)} %weight.1, ...), custom_call_target="tpu_custom_call" | custom-call | tf_op jit(solution)/shard_map/pallas_call | solution.py:358
  59.4 0.9 %copy.12 = f32[31,4,128]{2,1,0:T(4,128)S(1)} copy(f32[31,4,128]{2,0,1:T(8,128)} %bitcast.12) | data formatting | bytes 126976 | tf_op jit(solution)/shard_map/slice | solution.py:395
  60.3 0.6 copy.13
  60.9 1.3 %slice.14 = f32[1,4,128]{2,0,1:T(1,128)} slice(f32[32,4,128]{2,0,1:T(8,128)} %bitcast.13), slice={[31:32], [0:4], [0:128]} | slice | bytes 4096 | tf_op jit(solution)/shard_map/slice | solution.py:395
  62.2 0.0 copy-start
  62.2 2.4 %copy.19 = bf16[1024,512]{1,0:T(8,128)(2,1)} copy(bf16[1024,512]{1,0:T(8,128)(2,1)} %get-tuple-element.18) | data formatting | bytes 2097152
  64.6 0.0 copy-done
  64.6 0.0 copy-start.1
  64.6 1.0 %copy.20 = bf16[1024,512]{1,0:T(8,128)(2,1)} copy(bf16[1024,512]{1,0:T(8,128)(2,1)S(1)} %copy-done) | data formatting | bytes 2097152
  65.6 0.1 copy-done.1
  65.6 0.7 copy.21
  (1 shorter events, 0.0 us)
Async XLA Ops:
  62.2 2.4 %copy-start = (bf16[1024,512]{1,0:T(8,128)(2,1)S(1)}, bf16[1024,512]{1,0:T(8,128)(2,1)}, u32[]{:S(2)}) copy-start(bf16[1024,512]{1,0:T(8,128)(2,1)} %get-tuple-element.19) | copy-start | bytes 3145732
  64.6 1.0 %copy-start.1 = (f32[64,512]{1,0:T(8,128)S(1)}, f32[64,512]{1,0:T(8,128)}, u32[]{:S(2)}) copy-start(f32[64,512]{1,0:T(8,128)} %get-tuple-element.22) | copy-start | bytes 393220

commit v3 on v2

--- a/solution.py
+++ b/solution.py
@@ -100,12 +100,11 @@
             h - group_mean(h, matrix) - u * group_mean(hu, matrix))
 
 
-def taps_tile(c, dconv, gated, gain_part, sums):
-    kw = sums.shape[1] - 1
-    rows = dconv.shape[1] - 2 * EDGE
+def taps_tile(c, first, count, dconv, gated, tacc):
+    kw = tacc.shape[1]
 
     def chunk(r, accs):
-        at = r * 16
+        at = first + r * 16
         out = []
         d0 = dconv[c, pl.ds(pl.multiple_of(at + EDGE, 8), 8), :]
         d1 = dconv[c, pl.ds(pl.multiple_of(at + EDGE + 8, 8), 8), :]
@@ -115,9 +114,15 @@
             out.append(accs[k] + (d0 * g0 + d1 * g1))
         return tuple(out)
 
-    accs = lax.fori_loop(0, rows // 16, chunk, tuple(jnp.zeros((8, LANE), F32) for _ in range(kw)))
+    accs = lax.fori_loop(0, count // 16, chunk, tuple(tacc[c, k] for k in range(kw)))
     for k in range(kw):
-        sums[c, pl.ds(k, 1), :] = jnp.sum(accs[k], axis=0, keepdims=True)
+        tacc[c, k] = accs[k]
+
+
+def fold_taps(c, tacc, gain_part, sums):
+    kw = tacc.shape[1]
+    for k in range(kw):
+        sums[c, pl.ds(k, 1), :] = jnp.sum(tacc[c, k], axis=0, keepdims=True)
     sums[c, pl.ds(kw, 1), :] = jnp.sum(gain_part[:, lanes(c)], axis=0, keepdims=True)
 
 
@@ -149,8 +154,9 @@
     lax.fori_loop(lo, hi, one, 0)
 
 
-def whole_kernel(n, peers, value, gate, taps, gain, weight, grad,
-                 vgrad, ggrad, out_sums, wout,
+def whole_kernel(n, peers, value_in, gate_in, conv_taps, gain, weight_in, grad_in,
+                 vgrad_out, ggrad_out, taps_out, gain_out, wout,
+                 value, gate, weight, grad, vgrad, ggrad, taps, tacc, lsem, osem,
                  gated, unit, inv, normed, dconv, gain_part, wpart, sums,
                  vhalo, ohalo, others, send1, recv1, send2, recv2, send3, recv3,
                  arecv1, arecv2, asum, arecv3, atotal,
@@ -176,6 +182,10 @@
             src_ref=src, dst_ref=dst, send_sem=s, recv_sem=r, device_id=to,
             device_id_type=pl.DeviceIdType.MESH)
 
+    loads = [pltpu.make_async_copy(src, dst, lsem.at[i]) for i, (src, dst) in enumerate(
+        ((value_in, value), (gate_in, gate), (grad_in, grad), (weight_in, weight)))]
+    for copy in loads:
+        copy.start()
     barrier = pltpu.get_barrier_semaphore()
     friends = [(left, tmate(j)) for j in range(peers)] + [(right, tmate(j)) for j in range(peers)]
     friends += [(sp, tmate(j)) for j in range(1, peers)] + [(mate0, tp), (mate1, tp)]
@@ -188,12 +198,12 @@
     pending = []
     halos = []
     for side, (start, to) in enumerate(((rows - wide, right), (0, left))):
-        for i, ref in enumerate((value, gate)):
+        for i, ref in enumerate((value_in, gate_in)):
             halos.append(remote(ref.at[pl.ds(start, wide)], vhalo.at[side, i], vs.at[side, i], vr.at[side, i], (to, tp)))
     ohalos = []
     for side, (start, to) in enumerate(((rows - EDGE, right), (0, left))):
         for j in range(peers):
-            ohalos.append(remote(grad.at[pl.ds(start, EDGE)], ohalo.at[side, j], os_.at[side, j], or_.at[side, j], (to, tmate(j))))
+            ohalos.append(remote(grad_in.at[pl.ds(start, EDGE)], ohalo.at[side, j], os_.at[side, j], or_.at[side, j], (to, tmate(j))))
     for copy in halos + ohalos:
         copy.start()
     pending += halos + ohalos
@@ -202,7 +212,7 @@
 
     def gather(j, r):
         at = pl.ds(pl.multiple_of(r * step, step), step)
-        return remote(grad.at[at], others.at[j - 1, at], gs.at[j - 1, r], gr.at[j - 1, r], (sp, tmate(j)))
+        return remote(grad_in.at[at], others.at[j - 1, at], gs.at[j - 1, r], gr.at[j - 1, r], (sp, tmate(j)))
 
     for r in range(chunks):
         for j in range(1, peers):
@@ -211,6 +221,12 @@
             pending.append(copy)
 
     matrix = group_matrix()
+    for c in range(tiles):
+        taps[c] = conv_taps[:, c * LANE:(c + 1) * LANE].astype(F32)
+    gain_part[...] = jnp.zeros_like(gain_part)
+    tacc[...] = jnp.zeros_like(tacc)
+    loads[0].wait()
+    loads[1].wait()
     gstep = divisor(rows, 256, 32)
 
     def own_gated(c):
@@ -250,66 +266,118 @@
 
         loop(0, chans // piece, cols)
 
+    pairs, quads = n // 2 // peers, n // 4 // peers
+    span = group // peers
+
+    def half1(j):
+        at = pl.ds(lax.rem(tp + j, peers) * pairs, pairs)
+        return remote(send1.at[at], recv1.at[at], ws.at[0, j], wr.at[0, j], (mate0, tp))
+
+    def half2(j):
+        at = pl.ds(lax.rem(tp + j, peers) * quads, quads)
+        return remote(send2.at[at], recv2.at[at], ws.at[1, j], wr.at[1, j], (mate1, tp))
+
+    def start1(j):
+        first = lax.rem(tp + j, peers) * pairs
+
+        def cast(i):
+            send1[first + i] = wpart[2 * (first + i) + 1 - b0].astype(BF16)
+
+        loop(0, pairs, cast)
+        half1(j).start()
+
+    def start2(j):
+        first = lax.rem(tp + j, peers) * quads
+        half1(j).wait_recv()
+
+        def cast(i):
+            other, mine = 2 * (first + i) + 1 - b1, 2 * (first + i) + b1
+            send2[first + i] = (wpart[2 * other + b0] + recv1[other].astype(F32)).astype(BF16)
+            wpart[2 * mine + b0] = wpart[2 * mine + b0] + recv1[mine].astype(F32)
+
+        loop(0, quads, cast)
+        half2(j).start()
+
+    def total2(z):
+        return wpart[4 * z + 2 * b1 + b0] + recv2[z].astype(F32)
+
+    def final_copy(slot):
+        return remote(send3.at[slot], recv3.at[slot], ws3.at[slot], wr3.at[slot],
+                      (lax.rem(sp + 4 * (slot + 1), n), tp))
+
+    def start3(j):
+        half2(j).wait_recv()
+
+        def one(i):
+            z = lax.rem(tp + j, peers) * span + i
+            d = lax.rem(z + group - zz, group)
+
+            @pl.when(d != 0)
+            def _():
+                send3[d - 1] = total2(z).astype(BF16)
+                final_copy(d - 1).start()
+
+        loop(0, span, one)
+
+    def await_chunk(r):
+        for j in range(1, peers):
+            gather(j, r).wait_recv()
+
+    def middle(r):
+        at = pl.multiple_of(r * step, step)
+        ng = jnp.dot(grad[pl.ds(at, step), :], weight[owner(0), :], preferred_element_type=F32)
+        for j in range(1, peers):
+            ng += jnp.dot(others[j - 1, pl.ds(at, step), :], weight[owner(j), :], preferred_element_type=F32)
+        act_to_conv(ng, pl.multiple_of(at + EDGE, 8), step, True, unit, inv, gain, dconv, gain_part, matrix)
+
+    def taps_chunk(r):
+        loop(0, tiles, lambda c: taps_tile(c, pl.multiple_of(r * step, step), step, dconv, gated, tacc))
+
+    def both(r):
+        await_chunk(r)
+        middle(r)
+        taps_chunk(r)
+
+    def put_out(c):
+        backward_tile(c, dconv, value, gate, taps, vgrad, ggrad)
+        for copy in out_copies(c):
+            copy.start()
+
+    def out_copies(c):
+        return (pltpu.make_async_copy(vgrad.at[:, lanes(c)], vgrad_out.at[:, lanes(c)], osem.at[0, c]),
+                pltpu.make_async_copy(ggrad.at[:, lanes(c)], ggrad_out.at[:, lanes(c)], osem.at[1, c]))
+
+    loads[2].wait()
     weight_part(0)
-    gain_part[...] = jnp.zeros_like(gain_part)
+    start1(0)
+    loads[3].wait()
     for copy in ohalos:
         copy.wait_recv()
     for side, at in ((0, 0), (1, rows + EDGE)):
         ng = sum(jnp.dot(ohalo[side, j], weight[owner(j), :], preferred_element_type=F32) for j in range(peers))
         act_to_conv(ng * inside[side], at, EDGE, False, unit, inv, gain, dconv, gain_part, matrix)
-
-    def middle(r):
-        at = pl.multiple_of(r * step, step)
-        ng = jnp.dot(grad[pl.ds(at, step), :], weight[owner(0), :], preferred_element_type=F32)
-        for j in range(1, peers):
-            gather(j, r).wait_recv()
-            ng += jnp.dot(others[j - 1, pl.ds(at, step), :], weight[owner(j), :], preferred_element_type=F32)
-        act_to_conv(ng, pl.multiple_of(at + EDGE, 8), step, True, unit, inv, gain, dconv, gain_part, matrix)
-
-    loop(0, chunks, middle)
+    start2(0)
+    loop(0, chunks - 1, both)
+    start3(0)
+    await_chunk(chunks - 1)
     for j in range(1, peers):
         weight_part(j)
-
-    def cast1(a):
-        send1[a] = wpart[2 * a + 1 - b0].astype(BF16)
-
-    loop(0, n // 2, cast1)
-    copy1 = remote(send1, recv1, ws.at[0], wr.at[0], (mate0, tp))
-    copy1.start()
-    loop(0, half_tiles, lambda c: taps_tile(c, dconv, gated, gain_part, sums))
-    copy1.wait_recv()
-
-    def cast2(a):
-        other, mine = 2 * a + 1 - b1, 2 * a + b1
-        send2[a] = (wpart[2 * other + b0] + recv1[other].astype(F32)).astype(BF16)
-        wpart[2 * mine + b0] = wpart[2 * mine + b0] + recv1[mine].astype(F32)
-
-    loop(0, n // 4, cast2)
-    copy2 = remote(send2, recv2, ws.at[1], wr.at[1], (mate1, tp))
-    copy2.start()
-    loop(half_tiles, tiles, lambda c: taps_tile(c, dconv, gated, gain_part, sums))
+        start1(j)
+    middle(chunks - 1)
+    for j in range(1, peers):
+        start2(j)
+    taps_chunk(chunks - 1)
+    loop(0, tiles, lambda c: fold_taps(c, tacc, gain_part, sums))
 
     acopy1 = remote(sums.at[pl.ds((1 - b0) * half_tiles, half_tiles)], arecv1, as_.at[0], ar.at[0], (mate0, tp))
     acopy1.start()
     quarter = max(tiles // 4, 1)
-    loop(0, quarter, lambda c: backward_tile(c, dconv, value, gate, taps, vgrad, ggrad))
+    loop(0, quarter, put_out)
     acopy1.wait_recv()
     asum[0] = sums[pl.ds(b0 * half_tiles, half_tiles)] + arecv1[...]
     acopy2 = remote(asum.at[0], arecv2, as_.at[1], ar.at[1], (mate1, tp))
     acopy2.start()
-    copy2.wait_recv()
-
-    def total2(z):
-        return wpart[4 * z + 2 * b1 + b0] + recv2[z].astype(F32)
-
-    copies3 = []
-    for d in range(1, group):
-        send3[d - 1] = total2(lax.rem(zz + d, group)).astype(BF16)
-    for d in range(1, group):
-        copy = remote(send3.at[d - 1], recv3.at[d - 1], ws3.at[d - 1], wr3.at[d - 1], (zmate(d), tp))
-        copy.start()
-        copies3.append(copy)
-    loop(quarter, 2 * quarter, lambda c: backward_tile(c, dconv, value, gate, taps, vgrad, ggrad))
+    loop(quarter, 2 * quarter, put_out)
     acopy2.wait_recv()
     asum[1] = asum[0] + arecv2[...]
     acopies3 = []
@@ -317,7 +385,9 @@
         copy = remote(asum.at[1], arecv3.at[zz], as3.at[d - 1], ar3.at[d - 1], (zmate(d), tp))
         copy.start()
         acopies3.append(copy)
-    loop(2 * quarter, tiles, lambda c: backward_tile(c, dconv, value, gate, taps, vgrad, ggrad))
+    for j in range(1, peers):
+        start3(j)
+    loop(2 * quarter, tiles, put_out)
     for d in range(1, group):
         peer = lax.rem(zz + group - d, group)
         remote(asum.at[1], arecv3.at[peer], as3.at[d - 1], ar3.at[d - 1], (zmate(d), tp)).wait_recv()
@@ -330,13 +400,28 @@
     acopy4.start()
     final = total2(zz)
     for d in range(1, group):
-        copies3[d - 1].wait_recv()
+        final_copy(d - 1).wait_recv()
         final += recv3[d - 1].astype(F32)
     wout[...] = final
     remote(atotal.at[1 - b0], atotal.at[1 - b0], as_.at[2], ar.at[2], (mate0, tp)).wait_recv()
-    out_sums[...] = atotal[...].reshape(out_sums.shape)
-    for copy in pending + [copy1, copy2, acopy1, acopy2, acopy4] + copies3 + acopies3:
+    kw = tacc.shape[1]
+    for c in range(tiles):
+        tot = atotal[c // half_tiles, c % half_tiles]
+        taps_out[:, c * LANE:(c + 1) * LANE] = tot[:kw]
+        gain_out[:, c * LANE:(c + 1) * LANE] = tot[kw:]
+    for copy in pending + [acopy1, acopy2, acopy4] + acopies3:
         copy.wait_send()
+    for j in range(peers):
+        half1(j).wait_send()
+        half2(j).wait_send()
+    for d in range(1, group):
+        final_copy(d - 1).wait_send()
+
+    def drain(c):
+        for copy in out_copies(c):
+            copy.wait()
+
+    loop(0, tiles, drain)
 
 
 def per_device(value, gate, conv_taps, norm_gain, point_weight, out_grad):
@@ -348,19 +433,23 @@
     full = point_weight.shape[0]
     per = full // n
     group = n // 4
-    taps = conv_taps.astype(F32).reshape(kw, tiles, LANE).transpose(1, 0, 2)
     gain = norm_gain.reshape(1, chans)
-    args = (value, gate, taps, gain, point_weight, out_grad)
+    args = (value, gate, conv_taps, gain, point_weight, out_grad)
     half = (tiles // 2, kw + 1, LANE)
     vmem, dma = pltpu.VMEM, pltpu.SemaphoreType.DMA
     chunks = 4
-    outs = [((rows, chans), BF16), ((rows, chans), BF16), ((tiles, kw + 1, LANE), F32), ((per, chans), F32)]
-    vgrad, ggrad, sums, wgrad = pl.pallas_call(
+    outs = [((rows, chans), BF16), ((rows, chans), BF16), ((kw, chans), F32), ((1, chans), F32), ((per, chans), F32)]
+    vgrad, ggrad, taps_grad, gain_grad, wgrad = pl.pallas_call(
         functools.partial(whole_kernel, n, peers),
         out_shape=[jax.ShapeDtypeStruct(s, d) for s, d in outs],
-        in_specs=[pl.BlockSpec(memory_space=pltpu.VMEM)] * len(args),
-        out_specs=[pl.BlockSpec(memory_space=pltpu.VMEM)] * len(outs),
+        in_specs=[pl.BlockSpec(memory_space=m) for m in (pl.ANY, pl.ANY, vmem, vmem, pl.ANY, pl.ANY)],
+        out_specs=[pl.BlockSpec(memory_space=m) for m in (pl.ANY, pl.ANY, vmem, vmem, vmem)],
         scratch_shapes=[
+            vmem((rows, chans), BF16), vmem((rows, chans), BF16), vmem((full, chans), BF16), vmem((rows, chans), BF16),
+            vmem((rows, chans), BF16), vmem((rows, chans), BF16),
+            vmem((tiles, kw, LANE), F32),
+            vmem((tiles, kw, 8, LANE), F32),
+            dma((4,)), dma((2, tiles)),
             vmem((tiles, rows + 4 * EDGE, LANE), F32),
             vmem((tiles, extent, LANE), F32),
             vmem((tiles, extent, LANE), F32),
@@ -385,14 +474,13 @@
             vmem((2,) + half, F32),
             dma((2, 2)), dma((2, 2)), dma((2, peers)), dma((2, peers)),
             dma((peers - 1, chunks)), dma((peers - 1, chunks)),
-            dma((2,)), dma((2,)), dma((group - 1,)), dma((group - 1,)),
+            dma((2, peers)), dma((2, peers)), dma((group - 1,)), dma((group - 1,)),
             dma((3,)), dma((3,)), dma((group - 1,)), dma((group - 1,)),
         ],
         compiler_params=pltpu.CompilerParams(
             collective_id=0, has_side_effects=True, vmem_limit_bytes=56 * 1024 * 1024),
     )(*args)
-    flat = sums.transpose(1, 0, 2).reshape(kw + 1, chans)
-    return vgrad, ggrad, flat[:kw], flat[kw], wgrad
+    return vgrad, ggrad, taps_grad, gain_grad.reshape(chans), wgrad
 
 
 def solution(mesh):

time: 66.6 us -> 55 us (0.83)
  the two profiles are of different devices: /device:TPU:0 before, /device:TPU:24 now
where the time goes in v3:
time: 55 us; the launch traced here: 54.8 us
  Pallas kernels  48.9 us (89%)
  local copies, waits for them, and re-layouts  5.2 us (9%)
  between operations  0.65 us (1%)
    pallas_call x1, Pallas kernels, per_device(): pl.pallas_call(functools.partial(whole_kernel, n, peers), out_shape=[jax....  48.9 us
    unnamed x13, local copies, waits for them, and re-layouts  5.2 us

profile of v3, /device:TPU:24, one launch (start us, length us, event | category | flops | bytes accessed | tf_op | source)
XLA Modules:
  0.0 54.8 jit_solution(16880855008255587861)
XLA Ops:
  0.6 48.9 %shard_map.101 = (bf16[1024,512]{1,0:T(8,128)(2,1)}, bf16[1024,512]{1,0:T(8,128)(2,1)}, f32[31,512]{1,0:T(8,128)}, f32[1,512]{1,0:T(1,128)}, f32[64,512]{1,0:T(8,128)}) custom-call(bf16[1024,512]{1,0:T(8,128)(2,1)} %value_in.1, bf16[1024,512]{1,0:T(8,128)(2,1)} %gate_in.1, bf16[31,512]{1,0:T(8,128)(2,1)} %conv_taps.1, f32[1,512]{1,0:T(1,128)} %bitcast.2, ...), custom_call_target="tpu_custom_call" | custom-call | tf_op jit(solution)/shard_map/pallas_call | solution.py:442
  49.6 0.0 copy-start
  49.6 2.4 %copy.16 = bf16[1024,512]{1,0:T(8,128)(2,1)} copy(bf16[1024,512]{1,0:T(8,128)(2,1)} %get-tuple-element.20) | data formatting | bytes 2097152
  51.9 0.0 copy-done
  51.9 0.0 copy-start.2
  51.9 0.0 copy-start.3
  51.9 1.0 %copy.17 = bf16[1024,512]{1,0:T(8,128)(2,1)} copy(bf16[1024,512]{1,0:T(8,128)(2,1)S(1)} %copy-done) | data formatting | bytes 2097152
  52.9 0.0 copy-done.2
  52.9 0.0 copy-start.1
  52.9 0.6 %copy.18 = f32[31,512]{1,0:T(8,128)} copy(f32[31,512]{1,0:T(8,128)S(1)} %copy-done.2) | data formatting | bytes 126976
  53.5 0.0 copy-done.3
  53.5 0.6 %copy.19 = f32[512]{0:T(512)} copy(f32[512]{0:T(512)S(1)} %bitcast.3) | data formatting | bytes 4096
  54.1 0.0 copy-done.1
  54.1 0.7 %copy.20 = f32[64,512]{1,0:T(8,128)} copy(f32[64,512]{1,0:T(8,128)S(1)} %copy-done.1) | data formatting | bytes 262144
Async XLA Ops:
  49.6 2.4 %copy-start = (bf16[1024,512]{1,0:T(8,128)(2,1)S(1)}, bf16[1024,512]{1,0:T(8,128)(2,1)}, u32[]{:S(2)}) copy-start(bf16[1024,512]{1,0:T(8,128)(2,1)} %get-tuple-element.21) | copy-start | bytes 3145732
  51.9 1.0 %copy-start.2 = (f32[31,512]{1,0:T(8,128)S(1)}, f32[31,512]{1,0:T(8,128)}, u32[]{:S(2)}) copy-start(f32[31,512]{1,0:T(8,128)} %get-tuple-element.22) | copy-start | bytes 190468
  51.9 1.6 %copy-start.3 = (f32[1,512]{1,0:T(1,128)S(1)}, f32[1,512]{1,0:T(1,128)}, u32[]{:S(2)}) copy-start(f32[1,512]{1,0:T(1,128)} %get-tuple-element.13) | copy-start | bytes 6148
  52.9 1.2 %copy-start.1 = (f32[64,512]{1,0:T(8,128)S(1)}, f32[64,512]{1,0:T(8,128)}, u32[]{:S(2)}) copy-start(f32[64,512]{1,0:T(8,128)} %get-tuple-element.24) | copy-start | bytes 393220

commit v4 on v3

--- a/solution.py
+++ b/solution.py
@@ -36,6 +36,10 @@
     high = x.astype(BF16)
     low = (x - high.astype(F32)).astype(BF16)
     return jnp.dot(jnp.concatenate([high, low], axis=1), matrix, preferred_element_type=F32)
+
+
+def near_mean(x, matrix):
+    return jnp.dot(x.astype(BF16), matrix[:LANE], preferred_element_type=F32)
 
 
 def lanes(c):
@@ -67,7 +71,7 @@
         at = pl.multiple_of(r * nstep, 8)
         x = unit[c, pl.ds(at, nstep), :]
         centred = x - group_mean(x, matrix)
-        rs = lax.rsqrt(group_mean(centred * centred, matrix) + EPS)
+        rs = lax.rsqrt(near_mean(centred * centred, matrix) + EPS)
         inv[c, pl.ds(at, nstep), :] = rs
         unit[c, pl.ds(at, nstep), :] = centred * rs
         return 0
@@ -97,7 +101,7 @@
         h = a * g
         hu = au * g
         dconv[c, pl.ds(at, n), :] = inv[c, pl.ds(at, n), :] * (
-            h - group_mean(h, matrix) - u * group_mean(hu, matrix))
+            h - near_mean(h, matrix) - u * near_mean(hu, matrix))
 
 
 def taps_tile(c, first, count, dconv, gated, tacc):
@@ -422,6 +426,41 @@
             copy.wait()
 
     loop(0, tiles, drain)
+
+
+def finish_kernel(parts, *refs):
+    count = len(parts)
+    sources, targets, held = refs[:count], refs[count:2 * count], refs[2 * count:3 * count]
+    isem, osem = refs[3 * count:]
+    incoming, outgoing = [], []
+    slot = 0
+    for src, dst, buf, pieces in zip(sources, targets, held, parts):
+        size = src.shape[0] // pieces
+        for p in range(pieces):
+            at = pl.ds(p * size, size)
+            incoming.append(pltpu.make_async_copy(src.at[at], buf.at[at], isem.at[slot]))
+            outgoing.append(pltpu.make_async_copy(buf.at[at], dst.at[at], osem.at[slot]))
+            slot += 1
+    for copy in incoming:
+        copy.start()
+    for copy, after in zip(incoming, outgoing):
+        copy.wait()
+        after.start()
+    for copy in outgoing:
+        copy.wait()
+
+
+def finish(*arrays):
+    parts = [4 if a.shape[0] % 128 == 0 else 1 for a in arrays]
+    sems = pltpu.SemaphoreType.DMA((sum(parts),))
+    return pl.pallas_call(
+        functools.partial(finish_kernel, parts),
+        out_shape=[jax.ShapeDtypeStruct(a.shape, a.dtype) for a in arrays],
+        in_specs=[pl.BlockSpec(memory_space=pl.ANY)] * len(arrays),
+        out_specs=[pl.BlockSpec(memory_space=pl.ANY)] * len(arrays),
+        scratch_shapes=[pltpu.VMEM(a.shape, a.dtype) for a in arrays] + [sems, sems],
+        compiler_params=pltpu.CompilerParams(vmem_limit_bytes=60 * 1024 * 1024),
+    )(*arrays)
 
 
 def per_device(value, gate, conv_taps, norm_gain, point_weight, out_grad):
@@ -480,6 +519,7 @@
         compiler_params=pltpu.CompilerParams(
             collective_id=0, has_side_effects=True, vmem_limit_bytes=56 * 1024 * 1024),
     )(*args)
+    vgrad, ggrad, taps_grad, gain_grad, wgrad = finish(vgrad, ggrad, taps_grad, gain_grad, wgrad)
     return vgrad, ggrad, taps_grad, gain_grad.reshape(chans), wgrad
 
 

time: 55 us -> 52.2 us (0.949)
  local copies, waits for them, and re-layouts: 5.2 us -> 0 us
  Pallas kernels: 48.9 us -> 51.4 us
    unnamed x13 -> x0, local copies, waits for them, and re-layouts: 5.2 us -> none
    pallas_call x0 -> x1, Pallas kernels: none -> 2.51 us  [finish(): pl.pallas_call(functools.partial(finish_kernel, parts), out_shape=[jax.Sh...]
where the time goes in v4:
time: 52.2 us; the launch traced here: 52 us
  Pallas kernels  51.4 us (98%)
  between operations  0.64 us (1%)
    pallas_call x1, Pallas kernels, per_device(): pl.pallas_call(functools.partial(whole_kernel, n, peers), out_shape=[jax....  48.9 us
    pallas_call x1, Pallas kernels, finish(): pl.pallas_call(functools.partial(finish_kernel, parts), out_shape=[jax.Sh...  2.51 us

profile of v4, /device:TPU:24, one launch (start us, length us, event | category | flops | bytes accessed | tf_op | source)
XLA Modules:
  0.0 52.0 jit_solution(3691588222118122038)
XLA Ops:
  0.6 48.9 %shard_map.101 = (bf16[1024,512]{1,0:T(8,128)(2,1)}, bf16[1024,512]{1,0:T(8,128)(2,1)}, f32[31,512]{1,0:T(8,128)}, f32[1,512]{1,0:T(1,128)}, f32[64,512]{1,0:T(8,128)}) custom-call(bf16[1024,512]{1,0:T(8,128)(2,1)} %value_in.1, bf16[1024,512]{1,0:T(8,128)(2,1)} %gate_in.1, bf16[31,512]{1,0:T(8,128)(2,1)} %conv_taps.1, f32[1,512]{1,0:T(1,128)} %bitcast.2, ...), custom_call_target="tpu_custom_call" | custom-call | tf_op jit(solution)/shard_map/pallas_call | solution.py:481
  49.5 2.5 %shard_map.102 = (bf16[1024,512]{1,0:T(8,128)(2,1)}, bf16[1024,512]{1,0:T(8,128)(2,1)}, f32[31,512]{1,0:T(8,128)}, f32[1,512]{1,0:T(1,128)}, f32[64,512]{1,0:T(8,128)}) custom-call(bf16[1024,512]{1,0:T(8,128)(2,1)} %get-tuple-element.15.refs_0_, bf16[1024,512]{1,0:T(8,128)(2,1)} %get-tuple-element.16.refs_1_, f32[31,512]{1,0:T(8,128)} %get-tuple-element.17.refs_2_, ...), custom_call_target="tpu_custom_call" | custom-call | tf_op jit(solution)/shard_map/pallas_call | solution.py:456
